TPU v7x, 256 devices: a whole 4x4x8 slice. The times are simulated.
256 devices in a mesh: fs: 32 (over z, y), rep: 4 (over x), tp: 2 (over core).
Axes of the slice: x: 4, y: 4, z: 8, core: 2. Of those that a mesh axis runs over, the one named last changes fastest.
Arguments:
- saved_input: bfloat16 [131072, 2048], P(('fs', 'rep')), may hold values from -6 to 6
- cot_input: bfloat16 [131072, 1024], P(('fs', 'rep'), 'tp'), may hold values from -0.015625 to 0.015625
- cot_gate: bfloat16 [131072, 1024], P(('fs', 'rep'), 'tp'), may hold values from -0.015625 to 0.015625
- in_master: float32 [2048, 1024], P('fs', 'tp'), may hold values from -3 to 3
- gate_master: float32 [2048, 1024], P('fs', 'tp'), may hold values from -3 to 3
- in_factor: bfloat16 [2048, 256], P('fs'), may hold values from -0.125 to 0.125
- gate_factor: bfloat16 [2048, 256], P('fs'), may hold values from -0.125 to 0.125
- in_first: float32 [256, 1024], P('fs', 'tp'), may hold values from -6 to 6
- in_second: float32 [256, 1024], P('fs', 'tp'), may hold values from 0.5 to 2
- gate_first: float32 [256, 1024], P('fs', 'tp'), may hold values from -6 to 6
- gate_second: float32 [256, 1024], P('fs', 'tp'), may hold values from 0.5 to 2
Outputs:
- in_master_new: float32 [2048, 1024], P('fs', 'tp')
- gate_master_new: float32 [2048, 1024], P('fs', 'tp')
- in_update: float32 [2048, 1024], P('fs', 'tp')
- gate_update: float32 [2048, 1024], P('fs', 'tp')
- in_first_new: float32 [256, 1024], P('fs', 'tp')
- in_second_new: float32 [256, 1024], P('fs', 'tp')
- gate_first_new: float32 [256, 1024], P('fs', 'tp')
- gate_second_new: float32 [256, 1024], P('fs', 'tp')
- in_copy: bfloat16 [2048, 1024], P(None, 'tp')
- gate_copy: bfloat16 [2048, 1024], P(None, 'tp')
All inputs are finite; a program needn't handle non-finite values.
Results may differ from a plain program's by a relative error of at most 0.0065.
Values may be sent and summed in bfloat16 or wider, within the bound.
A program may use at most 64 MiB of HBM per device.

v0:
```python
import jax
import jax.numpy as jnp
from jax import lax
from jax.sharding import PartitionSpec as P

D = 2048
W = 1024


CONTRACT_ROWS = (((0,), (0,)), ((), ()))


def sent_together(arrays, axis, dim, along):
    ends, at = ([], 0)
    for a in arrays[:-1]:
        at += a.shape[along]
        ends.append(at)
    both = jnp.concatenate(arrays, axis=along)
    return tuple(jnp.split(lax.all_gather(both, axis, axis=dim, tiled=True), ends, axis=along))


def split_up(shard, dim, count):
    before, after = (shard.shape[:dim], shard.shape[dim + 1 :])
    return jnp.moveaxis(shard.reshape(*before, count, -1, *after), dim, 0)


def sent_and_summed(shard, axis, dim):
    count = lax.axis_size(axis)
    pieces = lax.all_to_all(split_up(shard, dim, count), axis, 0, 0, tiled=True)
    return jnp.sum(pieces.astype(jnp.float32), axis=0)


def sent_to_all(shard, axis):
    count = lax.axis_size(axis)
    return lax.all_to_all(
        jnp.broadcast_to(shard[None], (count, *shard.shape)), axis, 0, 0, tiled=True
    )


def of_everyone(shard, axis):
    return sent_to_all(shard, axis).astype(jnp.float32).sum(axis=0)


def joined_along(pieces, dim):
    dims = list(pieces.shape[1:])
    dims[dim] *= pieces.shape[0]
    return jnp.moveaxis(pieces, 0, dim).reshape(dims)


def collect(shard, axis, dim):
    return joined_along(sent_to_all(shard, axis), dim)


def of_everyone_2(shard, axis):
    return sent_to_all(shard, axis).sum(axis=0)


def in_one(arrays, axis):
    ravelled, at, gathered = (jnp.concatenate([a.reshape(-1) for a in arrays]), 0, [])
    running = of_everyone_2(ravelled, axis)
    for a in arrays:
        gathered.append(running[at : at + a.size].reshape(a.shape))
        at += a.size
    return tuple(gathered)


def plain_rows(left, right):
    return lax.dot_general(left, right, CONTRACT_ROWS, preferred_element_type=jnp.float32)


def split_parts(values):
    upper = values.astype(jnp.bfloat16)
    lower = (values - upper.astype(jnp.float32)).astype(jnp.bfloat16)
    return (upper, lower)


def on_device(
    saved_input,
    cot_input,
    cot_gate,
    in_master,
    gate_master,
    in_factor,
    gate_factor,
    in_first,
    in_second,
    gate_first,
    gate_second,
):
    width = in_master.shape[1]
    in_basis = in_factor.astype(jnp.float32)
    gate_basis = gate_factor.astype(jnp.float32)
    in_whole, gate_whole = sent_together((in_factor, gate_factor), "fs", 0, 1)
    in_upper, in_lower = split_parts(
        jnp.dot(saved_input, in_whole, preferred_element_type=jnp.float32)
    )
    gate_upper, gate_lower = split_parts(
        jnp.dot(saved_input, gate_whole, preferred_element_type=jnp.float32)
    )
    left = plain_rows(in_upper, cot_input)
    left = left + plain_rows(in_lower, cot_input)
    right = plain_rows(gate_upper, cot_gate)
    right = right + plain_rows(gate_lower, cot_gate)
    partial_low = sent_and_summed(
        jnp.concatenate([left, right], axis=1).astype(jnp.bfloat16), "fs", 0
    )
    low = of_everyone(partial_low.astype(jnp.bfloat16), "rep").astype(jnp.float32)
    first_old = jnp.concatenate([in_first, gate_first], axis=1)
    second_old = jnp.concatenate([in_second, gate_second], axis=1)
    first_new = 0.8 * first_old + 0.2 * low
    second_new = 0.95 * second_old + 0.05 * low * low
    normed = first_new / jnp.sqrt(second_new)
    piece = collect(normed, "fs", 0)
    left = jnp.dot(in_basis, piece[:, :width], precision=lax.Precision.HIGHEST)
    right = jnp.dot(gate_basis, piece[:, width:], precision=lax.Precision.HIGHEST)
    in_square, gate_square = in_one((jnp.sum(left * left), jnp.sum(right * right)), ("fs", "tp"))
    in_update = left / jnp.sqrt(in_square / (D * W) + 0.1)
    gate_update = right / jnp.sqrt(gate_square / (D * W) + 0.1)
    in_master_new = in_master - 0.05 * in_update
    gate_master_new = gate_master - 0.05 * gate_update
    in_copy, gate_copy = sent_together(
        (in_master_new.astype(jnp.bfloat16), gate_master_new.astype(jnp.bfloat16)), "fs", 0, 1
    )
    return (
        in_master_new,
        gate_master_new,
        in_update,
        gate_update,
        first_new[:, :width],
        second_new[:, :width],
        first_new[:, width:],
        second_new[:, width:],
        in_copy,
        gate_copy,
    )


def solution(mesh):
    placed = (
        P(("fs", "rep"), None),
        P(("fs", "rep"), "tp"),
        P(("fs", "rep"), "tp"),
        P("fs", "tp"),
        P("fs", "tp"),
        P("fs", None),
        P("fs", None),
        P("fs", "tp"),
        P("fs", "tp"),
        P("fs", "tp"),
        P("fs", "tp"),
    )
    return jax.shard_map(
        on_device,
        mesh=mesh,
        in_specs=placed,
        out_specs=(
            P("fs", "tp"),
            P("fs", "tp"),
            P("fs", "tp"),
            P("fs", "tp"),
            P("fs", "tp"),
            P("fs", "tp"),
            P("fs", "tp"),
            P("fs", "tp"),
            P(None, "tp"),
            P(None, "tp"),
        ),
        check_vma=False,
    )
```

profile of v0, /device:TPU:1, one launch (start us, length us, event | category | flops | bytes accessed | tf_op | source)
XLA Modules:
  0.0 261.1 jit_solution(14428039402485337618)
XLA Ops:
  7.2 0.0 copy-start
  7.2 0.0 all-gather.3.cloned.1.call-start
  7.2 1.5 pad_maximum_fusion.2
  8.7 0.0 all-gather.3.cloned.1.call-update
  8.8 0.0 all-gather.5.cloned.1.call-start
  8.8 79.5 %all-gather.3.cloned.1.call-done = bf16[2048,512]{1,0:T(8,128)(2,1)} async-done(((bf16[64,512]{1,0:T(8,128)(2,1)}), bf16[2048,512]{1,0:T(8,128)(2,1)}) %all-gather.3.cloned.1.call-update) | async-done | bytes 2097168 | tf_op jit(solution)/shard_map/all_gather | solution.py:19
  88.3 3.9 %convolution_bitcast_fusion.1 = f32[1024,256]{0,1:T(8,128)S(1)} fusion(bf16[1024,2048]{1,0:T(8,128)(2,1)} %param.11, bf16[2048,512]{1,0:T(8,128)(2,1)} %all-gather.3.cloned.1.call-done), kind=kOutput, calls=%fused_computation.1 | convolution fusion | flops 1073741824 | bytes 6291456 | tf_op jit(solution)/shard_map/dot_general | solution.py:95
  92.3 0.0 copy-done
  92.3 0.0 copy-start.10
  92.3 0.5 fusion.14
  92.8 0.5 fusion.3
  93.2 0.0 copy-done.11
  93.2 1.2 copy-done.10
  94.5 1.3 convolution_bitcast_fusion
  95.8 0.0 copy-done.1
  95.8 0.0 copy-start.6
  95.8 0.0 copy-start.7
  95.8 0.0 copy-start.8
  95.8 0.0 copy-start.9
  95.8 0.4 fusion.11
  96.3 0.0 copy-start.2
  96.3 0.4 fusion.2
  96.7 0.0 copy-start.3
  96.7 0.0 copy-start.4
  96.8 0.0 copy-start.5
  96.8 0.1 pad_maximum_fusion
  96.8 18.3 %all_to_all.21 = bf16[32,8,1024]{2,1,0:T(8,128)(2,1)S(1)} all-to-all(bf16[32,8,1024]{2,1,0:T(8,128)(2,1)S(1)} %pad_maximum_fusion), channel_id=1, replica_groups=mesh['fs'=32,'rep'=4,'tp'=2] {'fs'}, dimensions={0} | all-to-all | bytes 1048576 | tf_op jit(solution)/shard_map/all_to_all | solution.py:29
  115.1 0.1 reduce_sum.48
  115.2 8.2 %all_to_all.22 = bf16[4,8,1024]{2,1,0:T(8,128)(2,1)S(1)} all-to-all(bf16[4,8,1024]{2,1,0:T(8,128)(2,1)S(1)} %broadcast_in_dim.6), channel_id=1, replica_groups=mesh['fs'=32,'rep'=4,'tp'=2] {'rep'}, dimensions={0} | all-to-all | bytes 131072 | tf_op jit(solution)/shard_map/all_to_all | solution.py:35
  123.5 0.0 copy-done.6
  123.5 0.0 copy-done.7
  123.5 0.0 copy-done.8
  123.6 0.1 broadcast_in_dim.7
  123.7 23.4 %all_to_all.23 = f32[32,8,1024]{2,1,0:T(8,128)S(1)} all-to-all(f32[32,8,1024]{2,1,0:T(8,128)S(1)} %broadcast_in_dim.7), channel_id=1, replica_groups=mesh['fs'=32,'rep'=4,'tp'=2] {'fs'}, dimensions={0} | all-to-all | bytes 2097152 | tf_op jit(solution)/shard_map/all_to_all | solution.py:35
  147.1 0.9 multiply_reduce_fusion
  148.0 0.9 multiply_reduce_fusion.1
  149.0 1.4 pad_maximum_fusion.3
  150.4 24.6 %all_to_all.24 = f32[64,1,2]{2,1,0:T(1,128)S(1)} all-to-all(f32[64,1,2]{2,1,0:T(1,128)S(1)} %broadcast_in_dim.8), channel_id=1, replica_groups=mesh['fs'=32,'rep'=4,'tp'=2] {'fs','tp'}, dimensions={0} | all-to-all | bytes 1024 | tf_op jit(solution)/shard_map/all_to_all | solution.py:35
  175.0 0.1 reduce_sum.52
  175.1 0.6 fusion.25
  177.0 0.0 copy-done.4
  177.0 0.0 copy-done.5
  177.0 0.8 fusion.18
  177.9 0.7 pad_maximum_fusion.1
  178.5 0.0 all-gather.5.cloned.1.call-update
  178.6 0.6 fusion.23
  179.2 70.5 %all-gather.5.cloned.1.call-done = bf16[2048,1024]{1,0:T(8,128)(2,1)} async-done(((bf16[64,1024]{1,0:T(8,128)(2,1)}), bf16[2048,1024]{1,0:T(8,128)(2,1)}) %all-gather.5.cloned.1.call-update) | async-done | bytes 4194320 | tf_op jit(solution)/shard_map/all_gather | solution.py:19
  249.7 4.5 %fusion.22 = (bf16[2048,512]{1,0:T(8,128)(2,1)}, bf16[2048,512]{1,0:T(8,128)(2,1)}) fusion(bf16[2048,1024]{1,0:T(8,128)(2,1)} %all-gather.5.cloned.1.call-done), kind=kLoop, calls=%fused_computation.41 | loop fusion | bytes 8388608 | tf_op jit(solution)/shard_map/split | solution.py:19
  (9 shorter events, 0.1 us)
Async XLA Ops:
  7.2 85.1 %copy-start = (bf16[1024,512]{1,0:T(8,128)(2,1)S(1)}, bf16[1024,512]{1,0:T(8,128)(2,1)}, u32[]{:S(2)}) copy-start(bf16[1024,512]{1,0:T(8,128)(2,1)} %param.12) | copy-start | bytes 3145732
  7.2 81.1 %all-gather.3.cloned.1.call-start = ((), (), s32[]{:S(2)}) async-start(), calls=%async_computation.4 | async-start | bytes 2162688 | tf_op jit(solution)/shard_map/all_gather | solution.py:19
  8.8 241.0 %all-gather.5.cloned.1.call-start = ((), (), s32[]{:S(2)}) async-start(), calls=%async_computation.5 | async-start | bytes 4325376 | tf_op jit(solution)/shard_map/all_gather | solution.py:19
  88.3 4.9 %copy-start.11 = (bf16[2048,512]{1,0:T(8,128)(2,1)S(1)}, bf16[2048,512]{1,0:T(8,128)(2,1)}, u32[]{:S(2)}) copy-start(bf16[2048,512]{1,0:T(8,128)(2,1)} %all-gather.3.cloned.1.call-done) | copy-start | bytes 6291460
  92.3 2.2 copy-start.10
  94.5 1.3 copy-start.1
  95.8 27.7 %copy-start.6 = (f32[8,512]{1,0:T(8,128)S(1)}, f32[8,512]{1,0:T(8,128)}, u32[]{:S(2)}) copy-start(f32[8,512]{1,0:T(8,128)} %param.21) | copy-start | bytes 49156
  95.8 27.7 %copy-start.7 = (f32[8,512]{1,0:T(8,128)S(1)}, f32[8,512]{1,0:T(8,128)}, u32[]{:S(2)}) copy-start(f32[8,512]{1,0:T(8,128)} %param.19) | copy-start | bytes 49156
  95.8 27.7 %copy-start.8 = (f32[8,512]{1,0:T(8,128)S(1)}, f32[8,512]{1,0:T(8,128)}, u32[]{:S(2)}) copy-start(f32[8,512]{1,0:T(8,128)} %param.20) | copy-start | bytes 49156
  95.8 27.7 %copy-start.9 = (f32[8,512]{1,0:T(8,128)S(1)}, f32[8,512]{1,0:T(8,128)}, u32[]{:S(2)}) copy-start(f32[8,512]{1,0:T(8,128)} %param.18) | copy-start | bytes 49156
  96.3 50.8 %copy-start.2 = (bf16[64,256]{1,0:T(8,128)(2,1)S(1)}, bf16[64,256]{1,0:T(8,128)(2,1)}, u32[]{:S(2)}) copy-start(bf16[64,256]{1,0:T(8,128)(2,1)} %param.17) | copy-start | bytes 98308
  96.7 51.3 %copy-start.3 = (bf16[64,256]{1,0:T(8,128)(2,1)S(1)}, bf16[64,256]{1,0:T(8,128)(2,1)}, u32[]{:S(2)}) copy-start(bf16[64,256]{1,0:T(8,128)(2,1)} %param.16) | copy-start | bytes 98308
  96.7 80.3 %copy-start.4 = (f32[64,512]{1,0:T(8,128)S(1)}, f32[64,512]{1,0:T(8,128)}, u32[]{:S(2)}) copy-start(f32[64,512]{1,0:T(8,128)} %param.14) | copy-start | bytes 393220
  96.8 80.3 %copy-start.5 = (f32[64,512]{1,0:T(8,128)S(1)}, f32[64,512]{1,0:T(8,128)}, u32[]{:S(2)}) copy-start(f32[64,512]{1,0:T(8,128)} %param.15) | copy-start | bytes 393220
Sparse Core Ops, SparseCore 0:
  11.2 77.1 all-gather.2
  178.7 70.9 all-gather.4
where the time goes:
time: 264 us; the launch traced here: 261 us
  waiting for transfers between devices  150 us (57%)
  blocking collectives  74.5 us (28%)
  between operations  15.7 us (6%)
  matrix products  8.91 us (3%)
  local copies, waits for them, and re-layouts  7.17 us (3%)
  other arithmetic  4.6 us (2%)
    all_gather x2, waiting for transfers between devices, sent_together(): lax.all_gather(both, axis, axis=dim, tiled=True)  150 us
    all_to_all x3, blocking collectives, sent_to_all(): lax.all_to_all(jnp.broadcast_to(shard[None], (count, *shard.shape)), axis...  56.2 us
    all_to_all x1, blocking collectives, sent_and_summed(): pieces = lax.all_to_all(split_up(shard, dim, count), axis, 0, 0, tiled=True)  18.3 us
  transfers between devices with their start and end apart: 2, of which 2 were waited for; matrix products, arithmetic and copies ran while one was open for 0% of the time, Pallas kernels for 0%

commit v1 on v0

v1 whole, which is shorter than its diff:
```python
import jax
import jax.numpy as jnp
from jax import lax
from jax.experimental import pallas as pl
from jax.experimental.pallas import tpu as pltpu
from jax.sharding import PartitionSpec as P

D = 2048
W = 1024
RANK = 256
NX, NY, NZ = 4, 4, 8
ALPHA = 640
BF = jnp.bfloat16
F32 = jnp.float32
ANY = pl.ANY

XY = sorted(
    [(a, b) for a in range(4) for b in range(4) if (a, b) != (0, 0)],
    key=lambda o: -(min(o[0], 4 - o[0]) + min(o[1], 4 - o[1])),
)
ZD = sorted(range(1, 8), key=lambda d: -min(d, 8 - d))


def where_am_i():
    fs, x, c = lax.axis_index("fs"), lax.axis_index("rep"), lax.axis_index("tp")
    return x, lax.rem(fs, 4), lax.div(fs, 4), c


def remote(src, dst, ss, rs, dev):
    return pltpu.make_async_remote_copy(
        src_ref=src,
        dst_ref=dst,
        send_sem=ss,
        recv_sem=rs,
        device_id=dev,
        device_id_type=pl.DeviceIdType.MESH,
    )


def move_kernel(
    x_hbm, ci_hbm, cg_hbm, im_hbm, gm_hbm, if_hbm, gf_hbm, i1_hbm, i2_hbm, g1_hbm, g2_hbm,
    m_out, f_out, n_out, low_out, sq_out,
    xv, cot, cot_t, grad_t, fac, fsh, fall, mast, msh, mom_in, mom_own, mom,
    part, rsb, zb, nb, lowb, sqb,
    s_loc, fz_s, fz_r, mo_s, mo_r, mz_s, mz_r, fx_s, fx_r, ft_s, ft_r, my_s, my_r, mx_s, mx_r,
    rs_s, rs_r, zb_s, zb_r, lo_s, lo_r, ag_s, ag_r, sq_s, sq_r,
):
    x, y, z, c = where_am_i()

    def at(dx, dy, dz, dc=0):
        return {
            "fs": lax.rem(z + dz, 8) * 4 + lax.rem(y + dy, 4),
            "rep": lax.rem(x + dx, 4),
            "tp": lax.rem(c + dc, 2),
        }

    @pl.when(c == 0)
    def _():
        pltpu.make_async_copy(if_hbm, fac, s_loc.at[0]).start()

    @pl.when(c == 1)
    def _():
        pltpu.make_async_copy(gf_hbm, fac, s_loc.at[0]).start()

    moms = [
        pltpu.make_async_copy(r, mom_in.at[k], s_loc.at[1 + k])
        for k, r in enumerate((i1_hbm, g1_hbm, i2_hbm, g2_hbm))
    ]
    masters = [
        pltpu.make_async_copy(r, mast.at[k], s_loc.at[5 + k]) for k, r in enumerate((im_hbm, gm_hbm))
    ]
    cots = [
        pltpu.make_async_copy(r, cot.at[k], s_loc.at[7 + k]) for k, r in enumerate((ci_hbm, cg_hbm))
    ]
    load_x = pltpu.make_async_copy(x_hbm, xv, s_loc.at[9])
    for cp in (*moms, *masters, *cots, load_x):
        cp.start()

    barrier = pltpu.get_barrier_semaphore()
    peers = [at(a, b, 0) for a, b in XY] + [at(0, 0, d) for d in ZD] + [at(0, 0, 0, 1)]
    for p in peers:
        pl.semaphore_signal(barrier, inc=1, device_id=p, device_id_type=pl.DeviceIdType.MESH)

    pltpu.make_async_copy(if_hbm, fac, s_loc.at[0]).wait()
    new = lax.broadcasted_iota(jnp.int32, (RANK, RANK), 1)
    old = lax.broadcasted_iota(jnp.int32, (RANK, RANK), 0)
    ny, nz, ni = lax.shift_right_logical(new, 6), (lax.shift_right_logical(new, 3) & 7), new & 7
    perm = jnp.where(old == (nz * 4 + ny) * 8 + ni, 1.0, 0.0).astype(BF)
    shard = jnp.dot(fac[...], perm, preferred_element_type=F32).astype(BF)
    fsh[...] = shard.reshape(4, 16, RANK)
    fall[c, z, y, x] = fsh[x]

    for cp in moms:
        cp.wait()
    for q in range(4):
        kind, col = q // 2, (q % 2) * 256
        mom_own[q, 0] = mom_in[kind, :, col : col + 256]
        mom_own[q, 1] = mom_in[2 + kind, :, col : col + 256]
    mom[z] = mom_own[x]

    for cp in masters:
        cp.wait()
    msh[:, :512] = mast[0].astype(BF)
    msh[:, 512:] = mast[1].astype(BF)
    keep_m = pltpu.make_async_copy(msh, m_out.at[z, y], s_loc.at[10])
    keep_m.start()

    pl.semaphore_wait(barrier, len(peers))

    fz = [
        remote(fsh.at[x], fall.at[c, z, y, x], fz_s.at[k], fz_r.at[k], at(0, 0, d))
        for k, d in enumerate(ZD)
    ]
    mo = [remote(mom_own.at[x], mom.at[z], mo_s.at[k], mo_r.at[k], at(0, 0, d)) for k, d in enumerate(ZD)]
    mz = [remote(msh, m_out.at[z, y], mz_s.at[k], mz_r.at[k], at(0, 0, d)) for k, d in enumerate(ZD)]
    for cp in (*fz, *mo, *mz):
        cp.start()

    for cp in cots:
        cp.wait()
    for k in range(2):
        cot_t[k * 512 : (k + 1) * 512, :] = cot[k].T
    load_x.wait()

    def grad_step(i, _):
        cols = pl.ds(pl.multiple_of(i * 256, 256), 256)
        grad_t[:, cols] = jnp.dot(cot_t[...], xv[:, cols], preferred_element_type=F32).astype(BF)
        return 0

    lax.fori_loop(0, 2, grad_step, 0)

    for cp in fz:
        cp.wait_recv()
    fx = [
        remote(fall.at[c, :, y, x], fall.at[c, :, y, x], fx_s.at[k], fx_r.at[k], at(a, b, 0))
        for k, (a, b) in enumerate(XY)
    ]
    for cp in fx:
        cp.start()

    def to_partner(k, xs, ys):
        return remote(fall.at[c, :, ys, xs], fall.at[c, :, ys, xs], ft_s.at[k], ft_r.at[k], at(0, 0, 0, 1))

    ft = [to_partner(15, x, y)]
    ft[0].start()

    lax.fori_loop(2, 8, grad_step, 0)

    for k, (a, b) in reversed(list(enumerate(XY))):
        fx[k].wait_recv()
        cp = to_partner(k, lax.rem(x + 4 - a, 4), lax.rem(y + 4 - b, 4))
        cp.start()
        ft.append(cp)
    for cp in ft:
        cp.wait_recv()

    rs = []
    for dx in (2, 1, 3, 0):
        q = lax.rem(x + dx, 4)
        kind = lax.div(q, 2)
        basis = fall[kind].reshape(D, RANK)
        rows = pl.ds(pl.multiple_of(q * 256, 256), 256)
        low_t = jnp.dot(grad_t[rows, :], basis, preferred_element_type=F32)
        part[q] = low_t.T.astype(BF).reshape(4, 64, 256)
        for k, (a, b) in enumerate(XY):
            if a == dx:
                cp = remote(part.at[q, lax.rem(y + b, 4)], rsb.at[k], rs_s.at[k], rs_r.at[k], at(a, b, 0))
                cp.start()
                rs.append(cp)

    for cp in mz:
        cp.wait_recv()
    keep_m.wait()
    rows16 = pl.ds(pl.multiple_of(x * 16, 16), 16)
    my = []
    for k, b in enumerate((2, 1, 3)):
        whole = m_out.at[:, y, :, pl.ds(ALPHA, W - ALPHA)]
        quarter = m_out.at[:, y, rows16, pl.ds(0, ALPHA)]
        my.append(remote(quarter, quarter, my_s.at[2 * k], my_r.at[2 * k], at(0, b, 0)))
        my.append(remote(whole, whole, my_s.at[2 * k + 1], my_r.at[2 * k + 1], at(0, b, 0)))
    for cp in my:
        cp.start()

    keep_f = pltpu.make_async_copy(fall, f_out, s_loc.at[11])
    keep_f.start()

    grams = []
    for kind in range(2):
        basis = fall[kind].reshape(D, RANK)
        g = lax.dot_general(basis, basis, (((0,), (0,)), ((), ())), preferred_element_type=F32)
        hi = g.astype(BF)
        grams.append((hi, (g - hi.astype(F32)).astype(BF)))

    total = part[x, y].astype(F32)
    for cp in rs:
        cp.wait_recv()
    for k in range(15):
        total = total + rsb[k].astype(F32)
    zb[z] = total.astype(BF)
    zs = [remote(zb.at[z], zb.at[z], zb_s.at[k], zb_r.at[k], at(0, 0, d)) for k, d in enumerate(ZD)]
    for cp in zs:
        cp.start()
    for cp in mo:
        cp.wait_recv()
    first = mom[:, 0].reshape(64, 256)
    second = mom[:, 1].reshape(64, 256)
    for cp in zs:
        cp.wait_recv()
    low = zb[0].astype(F32)
    for k in range(1, 8):
        low = low + zb[k].astype(F32)
    first_new = 0.8 * first + 0.2 * low
    second_new = 0.95 * second + 0.05 * low * low
    nb[x, y] = (first_new / jnp.sqrt(second_new)).astype(BF)
    ag = [
        remote(nb.at[x, y], nb.at[x, y], ag_s.at[k], ag_r.at[k], at(a, b, 0))
        for k, (a, b) in enumerate(XY)
    ]
    for cp in ag:
        cp.start()

    part_low = low.reshape(8, 8, 256)
    mine = jnp.zeros((8, 256), F32)
    for k in range(8):
        mine = jnp.where(z == k, part_low[k], mine)
    lowb[x] = mine
    lo = [remote(lowb.at[x], lowb.at[x], lo_s.at[k], lo_r.at[k], at(a, 0, 0)) for k, a in enumerate((2, 1, 3))]
    for cp in lo:
        cp.start()

    for cp in my:
        cp.wait_recv()
    mx = []
    for k, a in enumerate((2, 1, 3)):
        for j in range(3):
            piece = m_out.at[:, lax.rem(y + 1 + j, 4), rows16, pl.ds(0, ALPHA)]
            mx.append(remote(piece, piece, mx_s.at[3 * k + j], mx_r.at[3 * k + j], at(a, 0, 0)))
    for cp in mx:
        cp.start()

    for cp in ag:
        cp.wait_recv()
    keep_n = pltpu.make_async_copy(nb, n_out, s_loc.at[12])
    keep_n.start()
    for kind in range(2):
        acc = jnp.zeros((8, 128), F32)
        for q in (2 * kind, 2 * kind + 1):
            normed = nb[q].reshape(RANK, 256)
            t = jnp.dot(grams[kind][0], normed, preferred_element_type=F32)
            t = t + jnp.dot(grams[kind][1], normed, preferred_element_type=F32)
            s = jnp.sum((t * normed.astype(F32)).reshape(32, 8, 256), axis=0)
            acc = acc + s[:, :128] + s[:, 128:]
        sqb[c, kind] = acc
    sq = remote(sqb.at[c], sqb.at[c], sq_s, sq_r, at(0, 0, 0, 1))
    sq.start()
    for cp in lo:
        cp.wait_recv()
    keep_low = pltpu.make_async_copy(lowb, low_out, s_loc.at[13])
    keep_low.start()
    sq.wait_recv()
    keep_sq = pltpu.make_async_copy(sqb, sq_out, s_loc.at[14])
    keep_sq.start()
    for cp in mx:
        cp.wait_recv()
    for cp in (*fz, *mo, *mz, *fx, *ft, *rs, *my, *zs, *ag, *lo, *mx, sq):
        cp.wait_send()
    for cp in (keep_f, keep_n, keep_low, keep_sq):
        cp.wait()


def gathered(x, ci, cg, im, gm, inf, gf, i1, i2, g1, g2):
    sem = pltpu.SemaphoreType.DMA
    return pl.pallas_call(
        move_kernel,
        name="move",
        out_shape=(
            jax.ShapeDtypeStruct((NZ, NY, 64, W), BF),
            jax.ShapeDtypeStruct((2, NZ, NY, NX, 16, RANK), BF),
            jax.ShapeDtypeStruct((NX, NY, 64, 256), BF),
            jax.ShapeDtypeStruct((NX, 8, 256), F32),
            jax.ShapeDtypeStruct((2, 2, 8, 128), F32),
        ),
        in_specs=[pl.BlockSpec(memory_space=ANY)] * 11,
        out_specs=[pl.BlockSpec(memory_space=ANY)] * 5,
        scratch_shapes=[
            pltpu.VMEM((1024, D), BF),
            pltpu.VMEM((2, 1024, 512), BF),
            pltpu.VMEM((1024, 1024), BF),
            pltpu.VMEM((1024, D), BF),
            pltpu.VMEM((64, RANK), BF),
            pltpu.VMEM((4, 16, RANK), BF),
            pltpu.VMEM((2, NZ, NY, NX, 16, RANK), BF),
            pltpu.VMEM((2, 64, 512), F32),
            pltpu.VMEM((64, W), BF),
            pltpu.VMEM((4, 8, 512), F32),
            pltpu.VMEM((4, 2, 8, 256), F32),
            pltpu.VMEM((NZ, 2, 8, 256), F32),
            pltpu.VMEM((NX, NY, 64, 256), BF),
            pltpu.VMEM((15, 64, 256), BF),
            pltpu.VMEM((NZ, 64, 256), BF),
            pltpu.VMEM((NX, NY, 64, 256), BF),
            pltpu.VMEM((NX, 8, 256), F32),
            pltpu.VMEM((2, 2, 8, 128), F32),
            sem((15,)),
            *[sem((n,)) for n in (7, 7, 7, 7, 7, 7, 15, 15, 16, 16, 6, 6, 9, 9, 15, 15, 7, 7, 3, 3, 15, 15)],
            sem,
            sem,
        ],
        compiler_params=pltpu.CompilerParams(
            collective_id=0, has_side_effects=True, vmem_limit_bytes=48 * 2**20
        ),
        cost_estimate=pl.CostEstimate(flops=6 * 10**9, bytes_accessed=16 * 2**20, transcendentals=0),
    )(x, ci, cg, im, gm, inf, gf, i1, i2, g1, g2)


def scales(sq):
    total = sq[0] + sq[1]
    return [lax.rsqrt(jnp.sum(total[k]) / (D * W) + 0.1) for k in range(2)]


def write_kernel(
    f_ref, n_ref, m_ref, sq_ref, low_ref, im_ref, gm_ref, i1_ref, i2_ref, g1_ref, g2_ref,
    im_out, gm_out, iu_out, gu_out, i1_out, i2_out, g1_out, g2_out, ic_out, gc_out,
):
    _, y, z, _ = where_am_i()
    step = pl.program_id(0)
    scale = scales(sq_ref[...])
    m = m_ref[...].reshape(256, W)
    for kind, out in enumerate((ic_out, gc_out)):
        basis = f_ref[kind].reshape(256, RANK)
        for h in range(2):
            normed = n_ref[2 * kind + h].reshape(RANK, 256)
            full = jnp.dot(basis, normed, preferred_element_type=F32)
            col = 256 * h
            old = m[:, kind * 512 + col : kind * 512 + col + 256].astype(F32)
            out[:, col : col + 256] = (old - 0.05 * (full * scale[kind])).astype(BF)

    @pl.when(step == z)
    def _():
        for kind, (old, new, upd) in enumerate(((im_ref, im_out, iu_out), (gm_ref, gm_out, gu_out))):
            basis = f_ref[kind, 0, y].reshape(64, RANK)
            for h in range(2):
                normed = n_ref[2 * kind + h].reshape(RANK, 256)
                cols = slice(256 * h, 256 * h + 256)
                u = jnp.dot(basis, normed, preferred_element_type=F32) * scale[kind]
                upd[:, cols] = u
                new[:, cols] = old[:, cols] - 0.05 * u

    @pl.when(step == 0)
    def _():
        for kind, (f_old, s_old, f_new, s_new) in enumerate(
            ((i1_ref, i2_ref, i1_out, i2_out), (g1_ref, g2_ref, g1_out, g2_out))
        ):
            for h in range(2):
                low = low_ref[2 * kind + h]
                cols = slice(256 * h, 256 * h + 256)
                f_new[:, cols] = 0.8 * f_old[:, cols] + 0.2 * low
                s_new[:, cols] = 0.95 * s_old[:, cols] + 0.05 * low * low


def written(f, n, m, sq, low, im, gm, i1, i2, g1, g2):
    def fixed(shape):
        return pl.BlockSpec(shape, lambda i: (0,) * len(shape))

    own, mo = fixed((64, 512)), fixed((8, 512))
    return pl.pallas_call(
        write_kernel,
        name="write",
        grid=(NZ,),
        out_shape=(
            *[jax.ShapeDtypeStruct((64, 512), F32)] * 4,
            *[jax.ShapeDtypeStruct((8, 512), F32)] * 4,
            *[jax.ShapeDtypeStruct((D, 512), BF)] * 2,
        ),
        in_specs=[
            pl.BlockSpec((2, 1, NY, NX, 16, RANK), lambda i: (0, i, 0, 0, 0, 0)),
            fixed((NX, NY, 64, 256)),
            pl.BlockSpec((1, NY, 64, W), lambda i: (i, 0, 0, 0)),
            fixed((2, 2, 8, 128)),
            fixed((NX, 8, 256)),
            own, own, mo, mo, mo, mo,
        ],
        out_specs=[own] * 4 + [mo] * 4 + [pl.BlockSpec((256, 512), lambda i: (i, 0))] * 2,
        compiler_params=pltpu.CompilerParams(dimension_semantics=("arbitrary",)),
    )(f, n, m, sq, low, im, gm, i1, i2, g1, g2)


def on_device(x, ci, cg, im, gm, inf, gf, i1, i2, g1, g2):
    m, f, n, low, sq = gathered(x, ci, cg, im, gm, inf, gf, i1, i2, g1, g2)
    out = written(f, n, m, sq, low, im, gm, i1, i2, g1, g2)
    return tuple(out)


def solution(mesh):
    tokens, rows, moments = P(("fs", "rep"), "tp"), P("fs", "tp"), P("fs", "tp")
    return jax.shard_map(
        on_device,
        mesh=mesh,
        in_specs=(
            P(("fs", "rep"), None), tokens, tokens, rows, rows, P("fs", None), P("fs", None),
            moments, moments, moments, moments,
        ),
        out_specs=(rows,) * 4 + (moments,) * 4 + (P(None, "tp"),) * 2,
        check_vma=False,
    )
```

time: 264 us -> 118 us (0.45)
  waiting for transfers between devices: 150 us -> 0 us
  Pallas kernels: 0 us -> 105 us
  blocking collectives: 74.5 us -> 0 us
  between operations: 15.7 us -> 0.68 us
  matrix products: 8.91 us -> 0 us
  local copies, waits for them, and re-layouts: 7.17 us -> 12 us
  other arithmetic: 4.6 us -> 0 us
    all_gather x2 -> x0, waiting for transfers between devices: 150 us -> none  [sent_together(): lax.all_gather(both, axis, axis=dim, tiled=True)]
    pallas_call x0 -> x2, Pallas kernels: none -> 105 us  [the longest x1 96.2 us: gathered(): pl.pallas_call(move_kernel, name='move', out_shape=(jax.ShapeDtypeStruct(...]
    all_to_all x4 -> x0, blocking collectives: 74.5 us -> none  [the longest x3 56.2 us: sent_to_all(): lax.all_to_all(jnp.broadcast_to(shard[None], (count, *shard.shape)), axis...]
    unnamed x24 -> x28, local copies, waits for them, and re-layouts: 1.32 us -> 12 us
    dot_general x8 -> x0, matrix products: 8.91 us -> none  [the longest x1 3.94 us: on_device(): jnp.dot(saved_input, in_whole, preferred_element_type=jnp.float32)]
    split x1 -> x0, local copies, waits for them, and re-layouts: 4.5 us -> none  [sent_together(): jnp.split(lax.all_gather(both, axis, axis=dim, tiled=True), ends, axis=al...]
    concatenate x4 -> x0, other arithmetic: 3.57 us -> none  [the longest x2 2.15 us: sent_together(): both = jnp.concatenate(arrays, axis=along)]
  transfers between devices with their start and end apart: 2 -> 0, of which waited for: 2 -> 0; matrix products, arithmetic and copies ran while one was open for 0% -> 0% of each run, Pallas kernels for 0% -> 0%
where the time goes in v1:
time: 118 us
  Pallas kernels  105 us (89%)
  local copies, waits for them, and re-layouts  12 us (10%)
    pallas_call x1, Pallas kernels, gathered(): pl.pallas_call(move_kernel, name='move', out_shape=(jax.ShapeDtypeStruct(...  96.2 us
    unnamed x28, local copies, waits for them, and re-layouts  12 us
    pallas_call x1, Pallas kernels, written(): pl.pallas_call(write_kernel, name='write', grid=(NZ,), out_shape=(*[jax.S...  8.79 us

profile of v1, /device:TPU:1, one launch (start us, length us, event | category | flops | bytes accessed | tf_op | source)
XLA Modules:
  0.0 117.7 jit_solution(15767828488282841813)
XLA Ops:
  0.6 0.0 copy-start.2
  0.7 0.9 copy-done.2
  1.6 0.0 copy-start.3
  1.6 0.9 copy-done.3
  2.5 0.0 copy-start.5
  2.5 0.7 copy-done.5
  3.2 0.0 copy-start.6
  3.2 0.7 copy-done.6
  3.9 0.0 copy-start.7
  3.9 0.7 copy-done.7
  4.6 0.0 copy-start.8
  4.6 0.7 copy-done.8
  5.3 0.0 copy-start.10
  5.3 1.2 %copy-done.10 = bf16[1024,512]{1,0:T(8,128)(2,1)S(1)} copy-done((bf16[1024,512]{1,0:T(8,128)(2,1)S(1)}, bf16[1024,512]{1,0:T(8,128)(2,1)}, u32[]{:S(2)}) %copy-start.10) | copy-done | bytes 1048600
  6.6 0.0 copy-start.11
  6.6 1.2 %copy-done.11 = bf16[1024,512]{1,0:T(8,128)(2,1)S(1)} copy-done((bf16[1024,512]{1,0:T(8,128)(2,1)S(1)}, bf16[1024,512]{1,0:T(8,128)(2,1)}, u32[]{:S(2)}) %copy-start.11) | copy-done | bytes 1048600
  7.8 0.0 copy-start.12
  7.8 0.8 copy-done.12
  8.5 0.0 copy-start.13
  8.5 0.8 copy-done.13
  9.3 96.2 %move.1 = (bf16[8,4,64,1024]{3,2,1,0:T(8,128)(2,1)}, bf16[2,8,4,4,16,256]{5,4,3,2,1,0:T(8,128)(2,1)S(1)}, bf16[4,4,64,256]{3,2,1,0:T(8,128)(2,1)S(1)}, f32[4,8,256]{2,1,0:T(8,128)S(1)}, f32[2,2,8,128]{3,2,1,0:T(8,128)S(1)}) custom-call(bf16[1024,2048]{1,0:T(8,128)(2,1)} %x_hbm.1, bf16[1024,512]{1,0:T(8,128)(2,1)S(1)} %copy-done.10, ...), custom_call_target="tpu_custom_call" | custom-call | flops 6000000000 | bytes 16777216 | tf_op jit(solution)/shard_map/move/pallas_call | solution.py:273
  105.5 0.0 copy-start
  105.5 1.3 %copy-done = bf16[2,8,4,4,16,256]{5,4,3,2,1,0:T(8,128)(2,1)} copy-done((bf16[2,8,4,4,16,256]{5,4,3,2,1,0:T(8,128)(2,1)}, bf16[2,8,4,4,16,256]{5,4,3,2,1,0:T(8,128)(2,1)S(1)}, u32[]{:S(2)}) %copy-start) | copy-done | bytes 2097176
  106.8 0.0 copy-start.1
  106.8 0.8 copy-done.1
  107.6 0.0 copy-start.4
  107.6 0.6 copy-done.4
  108.3 0.0 copy-start.9
  108.3 0.6 copy-done.9
  108.9 8.8 %write.1 = (f32[64,512]{1,0:T(8,128)}, f32[64,512]{1,0:T(8,128)}, f32[64,512]{1,0:T(8,128)}, f32[64,512]{1,0:T(8,128)}, f32[8,512]{1,0:T(8,128)}, /*index=5*/f32...) custom-call(bf16[2,8,4,4,16,256]{5,4,3,2,1,0:T(8,128)(2,1)} %copy-done, ...), custom_call_target="tpu_custom_call" | custom-call | tf_op jit(solution)/shard_map/write/pallas_call | solution.py:366
Async XLA Ops:
  0.6 0.9 copy-start.2
  1.6 0.9 copy-start.3
  2.5 0.7 copy-start.5
  3.2 0.7 copy-start.6
  3.9 0.7 copy-start.7
  4.6 0.7 copy-start.8
  5.3 1.2 %copy-start.10 = (bf16[1024,512]{1,0:T(8,128)(2,1)S(1)}, bf16[1024,512]{1,0:T(8,128)(2,1)}, u32[]{:S(2)}) copy-start(bf16[1024,512]{1,0:T(8,128)(2,1)} %ci_hbm.1) | copy-start | bytes 3145732
  6.6 1.2 %copy-start.11 = (bf16[1024,512]{1,0:T(8,128)(2,1)S(1)}, bf16[1024,512]{1,0:T(8,128)(2,1)}, u32[]{:S(2)}) copy-start(bf16[1024,512]{1,0:T(8,128)(2,1)} %cg_hbm.1) | copy-start | bytes 3145732
  7.8 0.8 copy-start.12
  8.5 0.8 copy-start.13
  105.5 1.3 %copy-start = (bf16[2,8,4,4,16,256]{5,4,3,2,1,0:T(8,128)(2,1)}, bf16[2,8,4,4,16,256]{5,4,3,2,1,0:T(8,128)(2,1)S(1)}, u32[]{:S(2)}) copy-start(bf16[2,8,4,4,16,256]{5,4,3,2,1,0:T(8,128)(2,1)S(1)} %get-tuple-element.15.f_ref) | copy-start | bytes 6291460
  106.8 0.8 copy-start.1
  107.6 0.6 copy-start.4
  108.3 0.6 copy-start.9

commit v2 on v1

--- a/solution.py
+++ b/solution.py
@@ -9,9 +9,10 @@
 W = 1024
 RANK = 256
 NX, NY, NZ = 4, 4, 8
-ALPHA = 640
+YZ_COLS, ZY_COLS, ZYX_COLS, Z_COLS = pl.ds(0, 384), pl.ds(384, 256), pl.ds(640, 384), pl.ds(384, 640)
 BF = jnp.bfloat16
 F32 = jnp.float32
+VMEM = 67_043_328
 ANY = pl.ANY
 
 XY = sorted(
@@ -42,7 +43,8 @@
     m_out, f_out, n_out, low_out, sq_out,
     xv, cot, cot_t, grad_t, fac, fsh, fall, mast, msh, mom_in, mom_own, mom,
     part, rsb, zb, nb, lowb, sqb,
-    s_loc, fz_s, fz_r, mo_s, mo_r, mz_s, mz_r, fx_s, fx_r, ft_s, ft_r, my_s, my_r, mx_s, mx_r,
+    s_loc, fz_s, fz_r, mo_s, mo_r, ra_s, ra_r, rb_s, rb_r, by_s, by_r, fx_s, fx_r, ft_s, ft_r,
+    my_s, my_r, mx_s, mx_r,
     rs_s, rs_r, zb_s, zb_r, lo_s, lo_r, ag_s, ag_r, sq_s, sq_r,
 ):
     x, y, z, c = where_am_i()
@@ -112,8 +114,39 @@
         for k, d in enumerate(ZD)
     ]
     mo = [remote(mom_own.at[x], mom.at[z], mo_s.at[k], mo_r.at[k], at(0, 0, d)) for k, d in enumerate(ZD)]
-    mz = [remote(msh, m_out.at[z, y], mz_s.at[k], mz_r.at[k], at(0, 0, d)) for k, d in enumerate(ZD)]
-    for cp in (*fz, *mo, *mz):
+    by = [
+        remote(msh.at[:, YZ_COLS], m_out.at[z, y, :, YZ_COLS], by_s.at[k], by_r.at[k], at(0, b, 0))
+        for k, b in enumerate((2, 1, 3))
+    ]
+
+    def ring(block, ss, rs):
+        hops = []
+        for h in range(4):
+            rows = (pl.ds(0, 32), pl.ds(32, 32)) if h == 3 else (pl.ds(0, 64),) * 2
+            up = block(lax.rem(z + 8 - h, 8), rows[0])
+            down = block(lax.rem(z + h, 8), rows[1])
+            hops.append(
+                (
+                    remote(up, up, ss.at[h, 0], rs.at[h, 0], at(0, 0, 1)),
+                    remote(down, down, ss.at[h, 1], rs.at[h, 1], at(0, 0, 7)),
+                )
+            )
+        return hops
+
+    def hop(hops, h):
+        if h:
+            for cp in hops[h - 1]:
+                cp.wait_recv()
+        for cp in hops[h]:
+            cp.start()
+
+    ra = ring(lambda k, rows: m_out.at[k, y, rows, Z_COLS], ra_s, ra_r)
+    rb = ring(lambda k, rows: m_out.at[k, :, rows, YZ_COLS], rb_s, rb_r)
+    for cp in (*fz, *by):
+        cp.start()
+    keep_m.wait()
+    hop(ra, 0)
+    for cp in mo:
         cp.start()
 
     for cp in cots:
@@ -144,15 +177,34 @@
     ft = [to_partner(15, x, y)]
     ft[0].start()
 
-    lax.fori_loop(2, 8, grad_step, 0)
+    lax.fori_loop(2, 4, grad_step, 0)
+    hop(ra, 1)
+    for cp in by:
+        cp.wait_recv()
+    hop(rb, 0)
+    lax.fori_loop(4, 8, grad_step, 0)
+    hop(ra, 2)
 
     for k, (a, b) in reversed(list(enumerate(XY))):
+        if k == 4:
+            hop(ra, 3)
+            hop(rb, 1)
         fx[k].wait_recv()
         cp = to_partner(k, lax.rem(x + 4 - a, 4), lax.rem(y + 4 - b, 4))
         cp.start()
         ft.append(cp)
     for cp in ft:
         cp.wait_recv()
+
+    for cp in ra[3]:
+        cp.wait_recv()
+    rows16 = pl.ds(pl.multiple_of(x * 16, 16), 16)
+    my = []
+    for k, b in enumerate((2, 1, 3)):
+        quarter = m_out.at[:, y, rows16, ZYX_COLS]
+        my.append(remote(quarter, quarter, my_s.at[k], my_r.at[k], at(0, b, 0)))
+    for cp in my:
+        cp.start()
 
     rs = []
     for dx in (2, 1, 3, 0):
@@ -168,17 +220,11 @@
                 cp.start()
                 rs.append(cp)
 
-    for cp in mz:
-        cp.wait_recv()
-    keep_m.wait()
-    rows16 = pl.ds(pl.multiple_of(x * 16, 16), 16)
-    my = []
+    mw = []
     for k, b in enumerate((2, 1, 3)):
-        whole = m_out.at[:, y, :, pl.ds(ALPHA, W - ALPHA)]
-        quarter = m_out.at[:, y, rows16, pl.ds(0, ALPHA)]
-        my.append(remote(quarter, quarter, my_s.at[2 * k], my_r.at[2 * k], at(0, b, 0)))
-        my.append(remote(whole, whole, my_s.at[2 * k + 1], my_r.at[2 * k + 1], at(0, b, 0)))
-    for cp in my:
+        whole = m_out.at[:, y, :, ZY_COLS]
+        mw.append(remote(whole, whole, my_s.at[3 + k], my_r.at[3 + k], at(0, b, 0)))
+    for cp in mw:
         cp.start()
 
     keep_f = pltpu.make_async_copy(fall, f_out, s_loc.at[11])
@@ -191,6 +237,7 @@
         hi = g.astype(BF)
         grams.append((hi, (g - hi.astype(F32)).astype(BF)))
 
+    hop(rb, 2)
     total = part[x, y].astype(F32)
     for cp in rs:
         cp.wait_recv()
@@ -200,6 +247,17 @@
     zs = [remote(zb.at[z], zb.at[z], zb_s.at[k], zb_r.at[k], at(0, 0, d)) for k, d in enumerate(ZD)]
     for cp in zs:
         cp.start()
+    for cp in my:
+        cp.wait_recv()
+    mx = []
+    for k, a in enumerate((2, 1, 3)):
+        for j in range(3):
+            piece = m_out.at[:, lax.rem(y + 1 + j, 4), rows16, ZYX_COLS]
+            mx.append(remote(piece, piece, mx_s.at[3 * k + j], mx_r.at[3 * k + j], at(a, 0, 0)))
+    for cp in mx:
+        cp.start()
+
+    hop(rb, 3)
     for cp in mo:
         cp.wait_recv()
     first = mom[:, 0].reshape(64, 256)
@@ -226,16 +284,6 @@
     lowb[x] = mine
     lo = [remote(lowb.at[x], lowb.at[x], lo_s.at[k], lo_r.at[k], at(a, 0, 0)) for k, a in enumerate((2, 1, 3))]
     for cp in lo:
-        cp.start()
-
-    for cp in my:
-        cp.wait_recv()
-    mx = []
-    for k, a in enumerate((2, 1, 3)):
-        for j in range(3):
-            piece = m_out.at[:, lax.rem(y + 1 + j, 4), rows16, pl.ds(0, ALPHA)]
-            mx.append(remote(piece, piece, mx_s.at[3 * k + j], mx_r.at[3 * k + j], at(a, 0, 0)))
-    for cp in mx:
         cp.start()
 
     for cp in ag:
@@ -260,9 +308,10 @@
     sq.wait_recv()
     keep_sq = pltpu.make_async_copy(sqb, sq_out, s_loc.at[14])
     keep_sq.start()
-    for cp in mx:
-        cp.wait_recv()
-    for cp in (*fz, *mo, *mz, *fx, *ft, *rs, *my, *zs, *ag, *lo, *mx, sq):
+    for cp in (*mw, *rb[3], *mx):
+        cp.wait_recv()
+    rings = [cp for h in (*ra, *rb) for cp in h]
+    for cp in (*fz, *mo, *by, *rings, *fx, *ft, *rs, *my, *mw, *zs, *ag, *lo, *mx, sq):
         cp.wait_send()
     for cp in (keep_f, keep_n, keep_low, keep_sq):
         cp.wait()
@@ -302,12 +351,14 @@
             pltpu.VMEM((NX, 8, 256), F32),
             pltpu.VMEM((2, 2, 8, 128), F32),
             sem((15,)),
-            *[sem((n,)) for n in (7, 7, 7, 7, 7, 7, 15, 15, 16, 16, 6, 6, 9, 9, 15, 15, 7, 7, 3, 3, 15, 15)],
+            *[sem((n,)) for n in (7, 7, 7, 7)],
+            *[sem((4, 2))] * 4,
+            *[sem((n,)) for n in (3, 3, 15, 15, 16, 16, 6, 6, 9, 9, 15, 15, 7, 7, 3, 3, 15, 15)],
             sem,
             sem,
         ],
         compiler_params=pltpu.CompilerParams(
-            collective_id=0, has_side_effects=True, vmem_limit_bytes=48 * 2**20
+            collective_id=0, has_side_effects=True, vmem_limit_bytes=VMEM
         ),
         cost_estimate=pl.CostEstimate(flops=6 * 10**9, bytes_accessed=16 * 2**20, transcendentals=0),
     )(x, ci, cg, im, gm, inf, gf, i1, i2, g1, g2)
@@ -321,10 +372,17 @@
 def write_kernel(
     f_ref, n_ref, m_ref, sq_ref, low_ref, im_ref, gm_ref, i1_ref, i2_ref, g1_ref, g2_ref,
     im_out, gm_out, iu_out, gu_out, i1_out, i2_out, g1_out, g2_out, ic_out, gc_out,
+    scale_ref,
 ):
     _, y, z, _ = where_am_i()
     step = pl.program_id(0)
-    scale = scales(sq_ref[...])
+
+    @pl.when(step == 0)
+    def _():
+        for kind, value in enumerate(scales(sq_ref[...])):
+            scale_ref[kind] = jnp.full((8, 128), value, F32)
+
+    scale = [scale_ref[kind, 0:1, 0:1] for kind in range(2)]
     m = m_ref[...].reshape(256, W)
     for kind, out in enumerate((ic_out, gc_out)):
         basis = f_ref[kind].reshape(256, RANK)
@@ -381,7 +439,10 @@
             own, own, mo, mo, mo, mo,
         ],
         out_specs=[own] * 4 + [mo] * 4 + [pl.BlockSpec((256, 512), lambda i: (i, 0))] * 2,
-        compiler_params=pltpu.CompilerParams(dimension_semantics=("arbitrary",)),
+        scratch_shapes=[pltpu.VMEM((2, 8, 128), F32)],
+        compiler_params=pltpu.CompilerParams(
+            dimension_semantics=("arbitrary",), vmem_limit_bytes=VMEM
+        ),
     )(f, n, m, sq, low, im, gm, i1, i2, g1, g2)
 
 

time: 118 us -> 78.2 us (0.66)
  Pallas kernels: 105 us -> 77.3 us
  local copies, waits for them, and re-layouts: 12 us -> 0 us
    pallas_call x1, Pallas kernels: 96.2 us -> 68.3 us  [gathered(): pl.pallas_call(move_kernel, name='move', out_shape=(jax.ShapeDtypeStruct(...]
    unnamed x28 -> x0, local copies, waits for them, and re-layouts: 12 us -> none
where the time goes in v2:
time: 78.2 us; the launch traced here: 77.9 us
  Pallas kernels  77.3 us (99%)
    pallas_call x1, Pallas kernels, gathered(): pl.pallas_call(move_kernel, name='move', out_shape=(jax.ShapeDtypeStruct(...  68.3 us
    pallas_call x1, Pallas kernels, written(): pl.pallas_call(write_kernel, name='write', grid=(NZ,), out_shape=(*[jax.S...  8.94 us

profile of v2, /device:TPU:1, one launch (start us, length us, event | category | flops | bytes accessed | tf_op | source)
XLA Modules:
  0.0 77.9 jit_solution(2077084683354148522)
XLA Ops:
  0.6 68.3 %move.1 = (bf16[8,4,64,1024]{3,2,1,0:T(8,128)(2,1)}, bf16[2,8,4,4,16,256]{5,4,3,2,1,0:T(8,128)(2,1)}, bf16[4,4,64,256]{3,2,1,0:T(8,128)(2,1)}, f32[4,8,256]{2,1,0:T(8,128)}, f32[2,2,8,128]{3,2,1,0:T(8,128)}) custom-call(bf16[1024,2048]{1,0:T(8,128)(2,1)} %x_hbm.1, bf16[1024,512]{1,0:T(8,128)(2,1)} %ci_hbm.1, bf16[1024,512]{1,0:T(8,128)(2,1)} %cg_hbm.1, ...), custom_call_target="tpu_custom_call" | custom-call | flops 6000000000 | bytes 16777216 | tf_op jit(solution)/shard_map/move/pallas_call | solution.py:322
  69.0 8.9 %write.1 = (f32[64,512]{1,0:T(8,128)}, f32[64,512]{1,0:T(8,128)}, f32[64,512]{1,0:T(8,128)}, f32[64,512]{1,0:T(8,128)}, f32[8,512]{1,0:T(8,128)}, /*index=5*/f32...) custom-call(bf16[2,8,4,4,16,256]{5,4,3,2,1,0:T(8,128)(2,1)} %get-tuple-e, ...), custom_call_target="tpu_custom_call" | custom-call | tf_op jit(solution)/shard_map/write/pallas_call | solution.py:424

commit v3 on v2

--- a/solution.py
+++ b/solution.py
@@ -9,7 +9,10 @@
 W = 1024
 RANK = 256
 NX, NY, NZ = 4, 4, 8
-YZ_COLS, ZY_COLS, ZYX_COLS, Z_COLS = pl.ds(0, 384), pl.ds(384, 256), pl.ds(640, 384), pl.ds(384, 640)
+YZ_COLS, YZ0, YZ1 = pl.ds(0, 512), pl.ds(0, 256), pl.ds(256, 256)
+ZY_COLS, ZYX_COLS, Z_COLS = pl.ds(512, 128), pl.ds(640, 384), pl.ds(512, 512)
+HERE = 3
+NEAR, BELOW, ABOVE = pl.ds(2, 3), pl.ds(0, 2), pl.ds(5, 3)
 BF = jnp.bfloat16
 F32 = jnp.float32
 VMEM = 67_043_328
@@ -43,7 +46,8 @@
     m_out, f_out, n_out, low_out, sq_out,
     xv, cot, cot_t, grad_t, fac, fsh, fall, mast, msh, mom_in, mom_own, mom,
     part, rsb, zb, nb, lowb, sqb,
-    s_loc, fz_s, fz_r, mo_s, mo_r, ra_s, ra_r, rb_s, rb_r, by_s, by_r, fx_s, fx_r, ft_s, ft_r,
+    s_loc, fz_s, fz_r, mo_s, mo_r, ra_s, ra_r, rb_s, rb_r, rc_s, rc_r, by_s, by_r, fa_s, fa_r, fb_s, fb_r,
+    fc_s, fc_r, fd_s, fd_r, ft_s, ft_r,
     my_s, my_r, mx_s, mx_r,
     rs_s, rs_r, zb_s, zb_r, lo_s, lo_r, ag_s, ag_r, sq_s, sq_r,
 ):
@@ -104,7 +108,7 @@
         cp.wait()
     msh[:, :512] = mast[0].astype(BF)
     msh[:, 512:] = mast[1].astype(BF)
-    keep_m = pltpu.make_async_copy(msh, m_out.at[z, y], s_loc.at[10])
+    keep_m = pltpu.make_async_copy(msh, m_out.at[HERE, y], s_loc.at[10])
     keep_m.start()
 
     pl.semaphore_wait(barrier, len(peers))
@@ -115,20 +119,20 @@
     ]
     mo = [remote(mom_own.at[x], mom.at[z], mo_s.at[k], mo_r.at[k], at(0, 0, d)) for k, d in enumerate(ZD)]
     by = [
-        remote(msh.at[:, YZ_COLS], m_out.at[z, y, :, YZ_COLS], by_s.at[k], by_r.at[k], at(0, b, 0))
+        remote(msh.at[:, YZ_COLS], m_out.at[HERE, y, :, YZ_COLS], by_s.at[k], by_r.at[k], at(0, b, 0))
         for k, b in enumerate((2, 1, 3))
     ]
 
     def ring(block, ss, rs):
         hops = []
         for h in range(4):
-            rows = (pl.ds(0, 32), pl.ds(32, 32)) if h == 3 else (pl.ds(0, 64),) * 2
-            up = block(lax.rem(z + 8 - h, 8), rows[0])
-            down = block(lax.rem(z + h, 8), rows[1])
+            lower, upper = (pl.ds(0, 32), pl.ds(32, 32)) if h == 3 else (pl.ds(0, 64),) * 2
+            up = (block(HERE - h, lower), block(HERE - h - 1 if h < 3 else HERE + 4, lower))
+            down = (block(HERE + h, upper), block(HERE + h + 1, upper))
             hops.append(
                 (
-                    remote(up, up, ss.at[h, 0], rs.at[h, 0], at(0, 0, 1)),
-                    remote(down, down, ss.at[h, 1], rs.at[h, 1], at(0, 0, 7)),
+                    remote(*up, ss.at[h, 0], rs.at[h, 0], at(0, 0, 1)),
+                    remote(*down, ss.at[h, 1], rs.at[h, 1], at(0, 0, 7)),
                 )
             )
         return hops
@@ -141,13 +145,47 @@
             cp.start()
 
     ra = ring(lambda k, rows: m_out.at[k, y, rows, Z_COLS], ra_s, ra_r)
-    rb = ring(lambda k, rows: m_out.at[k, :, rows, YZ_COLS], rb_s, rb_r)
+    rb = ring(lambda k, rows: m_out.at[k, :, rows, YZ0], rb_s, rb_r)
+    rc = ring(lambda k, rows: m_out.at[k, :, rows, YZ1], rc_s, rc_r)
     for cp in (*fz, *by):
         cp.start()
     keep_m.wait()
     hop(ra, 0)
-    for cp in mo:
-        cp.start()
+
+    rows16 = pl.ds(pl.multiple_of(x * 16, 16), 16)
+    part_of = {"near": NEAR, "below": BELOW, "above": ABOVE}
+
+    def along_y(group, rows, cols, first):
+        block = m_out.at[part_of[group], y, rows, cols]
+        return [
+            remote(block, block, my_s.at[first + k], my_r.at[first + k], at(0, b, 0))
+            for k, b in enumerate((2, 1, 3))
+        ]
+
+    def along_x(group, first):
+        out = []
+        for k, a in enumerate((2, 1, 3)):
+            for j in range(3):
+                block = m_out.at[part_of[group], lax.rem(y + 1 + j, 4), rows16, ZYX_COLS]
+                n = first + 3 * k + j
+                out.append(remote(block, block, mx_s.at[n], mx_r.at[n], at(a, 0, 0)))
+        return out
+
+    every = pl.ds(0, 64)
+    groups = ("near", "below", "above")
+    quarters = {g: along_y(g, rows16, ZYX_COLS, 3 * k) for k, g in enumerate(groups)}
+    wholes = {g: along_y(g, every, ZY_COLS, 9 + 3 * k) for k, g in enumerate(groups)}
+    acrosses = {g: along_x(g, 9 * k) for k, g in enumerate(groups)}
+
+    def start(*lists):
+        for cps in lists:
+            for cp in cps:
+                cp.start()
+
+    def arrive(*lists):
+        for cps in lists:
+            for cp in cps:
+                cp.wait_recv()
 
     for cp in cots:
         cp.wait()
@@ -164,47 +202,82 @@
 
     for cp in fz:
         cp.wait_recv()
-    fx = [
-        remote(fall.at[c, :, y, x], fall.at[c, :, y, x], fx_s.at[k], fx_r.at[k], at(a, b, 0))
-        for k, (a, b) in enumerate(XY)
-    ]
-    for cp in fx:
-        cp.start()
-
-    def to_partner(k, xs, ys):
-        return remote(fall.at[c, :, ys, xs], fall.at[c, :, ys, xs], ft_s.at[k], ft_r.at[k], at(0, 0, 0, 1))
-
-    ft = [to_partner(15, x, y)]
-    ft[0].start()
+    def piece(half, xs, ys):
+        return fall.at[c, pl.ds(4 * half, 4), ys, xs]
+
+    def send_piece(half, xs, ys, ss, rs, dev):
+        block = piece(half, xs, ys)
+        return remote(block, block, ss, rs, dev)
+
+    def back(p, d):
+        return lax.rem(p + 4 - d, 4)
+
+    near = (1, 3, 2)
+    fa = [send_piece(0, x, y, fa_s.at[k], fa_r.at[k], at(0, b, 0)) for k, b in enumerate(near)]
+    fb = [send_piece(1, x, y, fb_s.at[k], fb_r.at[k], at(a, 0, 0)) for k, a in enumerate(near)]
+    ysrc = [y] + [back(y, b) for b in near]
+    xsrc = [x] + [back(x, a) for a in near]
+    fc = [
+        [send_piece(0, x, ys, fc_s.at[i, k], fc_r.at[i, k], at(a, 0, 0)) for k, a in enumerate(near)]
+        for i, ys in enumerate(ysrc)
+    ]
+    fd = [
+        [send_piece(1, xs, y, fd_s.at[i, k], fd_r.at[i, k], at(0, b, 0)) for k, b in enumerate(near)]
+        for i, xs in enumerate(xsrc)
+    ]
+    ft = []
+
+    def to_partner(half, xs, ys):
+        k = len(ft)
+        cp = send_piece(half, xs, ys, ft_s.at[k], ft_r.at[k], at(0, 0, 0, 1))
+        cp.start()
+        ft.append(cp)
+
+    start(fa, fb, fc[0], fd[0])
+    to_partner(0, x, y)
+    to_partner(1, x, y)
 
     lax.fori_loop(2, 4, grad_step, 0)
     hop(ra, 1)
-    for cp in by:
-        cp.wait_recv()
+    start(quarters["near"])
+    arrive(by)
     hop(rb, 0)
-    lax.fori_loop(4, 8, grad_step, 0)
+
+    def relay(k):
+        fa[k].wait_recv()
+        start(fc[1 + k])
+        fb[k].wait_recv()
+        start(fd[1 + k])
+        to_partner(0, x, ysrc[1 + k])
+        to_partner(1, xsrc[1 + k], y)
+
+    relay(0)
+    relay(1)
+    lax.fori_loop(4, 5, grad_step, 0)
+    relay(2)
     hop(ra, 2)
-
-    for k, (a, b) in reversed(list(enumerate(XY))):
-        if k == 4:
-            hop(ra, 3)
-            hop(rb, 1)
-        fx[k].wait_recv()
-        cp = to_partner(k, lax.rem(x + 4 - a, 4), lax.rem(y + 4 - b, 4))
-        cp.start()
-        ft.append(cp)
-    for cp in ft:
-        cp.wait_recv()
-
-    for cp in ra[3]:
-        cp.wait_recv()
-    rows16 = pl.ds(pl.multiple_of(x * 16, 16), 16)
-    my = []
-    for k, b in enumerate((2, 1, 3)):
-        quarter = m_out.at[:, y, rows16, ZYX_COLS]
-        my.append(remote(quarter, quarter, my_s.at[k], my_r.at[k], at(0, b, 0)))
-    for cp in my:
-        cp.start()
+    hop(rc, 0)
+    lax.fori_loop(5, 7, grad_step, 0)
+
+    def land(i):
+        for k in range(3):
+            fc[i][k].wait_recv()
+            to_partner(0, xsrc[1 + k], ysrc[i])
+            fd[i][k].wait_recv()
+            to_partner(1, xsrc[i], ysrc[1 + k])
+
+    land(0)
+    arrive(quarters["near"])
+    start(acrosses["near"], wholes["near"])
+    hop(ra, 3)
+    lax.fori_loop(7, 8, grad_step, 0)
+    hop(rb, 1)
+    hop(rc, 1)
+    land(1)
+    land(2)
+    start(mo)
+    land(3)
+    arrive(ft)
 
     rs = []
     for dx in (2, 1, 3, 0):
@@ -220,12 +293,10 @@
                 cp.start()
                 rs.append(cp)
 
-    mw = []
-    for k, b in enumerate((2, 1, 3)):
-        whole = m_out.at[:, y, :, ZY_COLS]
-        mw.append(remote(whole, whole, my_s.at[3 + k], my_r.at[3 + k], at(0, b, 0)))
-    for cp in mw:
-        cp.start()
+    arrive(ra[3])
+    start(quarters["below"], quarters["above"])
+    hop(rb, 2)
+    hop(rc, 2)
 
     keep_f = pltpu.make_async_copy(fall, f_out, s_loc.at[11])
     keep_f.start()
@@ -237,7 +308,7 @@
         hi = g.astype(BF)
         grams.append((hi, (g - hi.astype(F32)).astype(BF)))
 
-    hop(rb, 2)
+    start(wholes["below"], wholes["above"])
     total = part[x, y].astype(F32)
     for cp in rs:
         cp.wait_recv()
@@ -247,17 +318,11 @@
     zs = [remote(zb.at[z], zb.at[z], zb_s.at[k], zb_r.at[k], at(0, 0, d)) for k, d in enumerate(ZD)]
     for cp in zs:
         cp.start()
-    for cp in my:
-        cp.wait_recv()
-    mx = []
-    for k, a in enumerate((2, 1, 3)):
-        for j in range(3):
-            piece = m_out.at[:, lax.rem(y + 1 + j, 4), rows16, ZYX_COLS]
-            mx.append(remote(piece, piece, mx_s.at[3 * k + j], mx_r.at[3 * k + j], at(a, 0, 0)))
-    for cp in mx:
-        cp.start()
-
     hop(rb, 3)
+    arrive(quarters["above"])
+    start(acrosses["above"])
+    hop(rc, 3)
+    arrive(quarters["below"])
     for cp in mo:
         cp.wait_recv()
     first = mom[:, 0].reshape(64, 256)
@@ -276,6 +341,8 @@
     ]
     for cp in ag:
         cp.start()
+
+    start(acrosses["below"])
 
     part_low = low.reshape(8, 8, 256)
     mine = jnp.zeros((8, 256), F32)
@@ -308,10 +375,11 @@
     sq.wait_recv()
     keep_sq = pltpu.make_async_copy(sqb, sq_out, s_loc.at[14])
     keep_sq.start()
-    for cp in (*mw, *rb[3], *mx):
-        cp.wait_recv()
-    rings = [cp for h in (*ra, *rb) for cp in h]
-    for cp in (*fz, *mo, *by, *rings, *fx, *ft, *rs, *my, *mw, *zs, *ag, *lo, *mx, sq):
+    arrive(rb[3], rc[3], *wholes.values(), *acrosses.values())
+    rings = [cp for h in (*ra, *rb, *rc) for cp in h]
+    spread = [cp for d in (quarters, wholes, acrosses) for cps in d.values() for cp in cps]
+    relays = [cp for cps in (*fc, *fd) for cp in cps]
+    for cp in (*fz, *mo, *by, *rings, *fa, *fb, *relays, *ft, *rs, *spread, *zs, *ag, *lo, sq):
         cp.wait_send()
     for cp in (keep_f, keep_n, keep_low, keep_sq):
         cp.wait()
@@ -352,8 +420,10 @@
             pltpu.VMEM((2, 2, 8, 128), F32),
             sem((15,)),
             *[sem((n,)) for n in (7, 7, 7, 7)],
-            *[sem((4, 2))] * 4,
-            *[sem((n,)) for n in (3, 3, 15, 15, 16, 16, 6, 6, 9, 9, 15, 15, 7, 7, 3, 3, 15, 15)],
+            *[sem((4, 2))] * 6,
+            *[sem((3,))] * 6,
+            *[sem((4, 3))] * 4,
+            *[sem((n,)) for n in (32, 32, 18, 18, 27, 27, 15, 15, 7, 7, 3, 3, 15, 15)],
             sem,
             sem,
         ],
@@ -364,85 +434,91 @@
     )(x, ci, cg, im, gm, inf, gf, i1, i2, g1, g2)
 
 
-def scales(sq):
-    total = sq[0] + sq[1]
-    return [lax.rsqrt(jnp.sum(total[k]) / (D * W) + 0.1) for k in range(2)]
-
-
 def write_kernel(
-    f_ref, n_ref, m_ref, sq_ref, low_ref, im_ref, gm_ref, i1_ref, i2_ref, g1_ref, g2_ref,
+    f_hbm, n_hbm, m_hbm, sq_hbm, low_ref, im_ref, gm_ref, i1_ref, i2_ref, g1_ref, g2_ref,
     im_out, gm_out, iu_out, gu_out, i1_out, i2_out, g1_out, g2_out, ic_out, gc_out,
-    scale_ref,
+    fv, nv, mv, sqv, cv, s_f, s_n, s_m, s_c,
 ):
     _, y, z, _ = where_am_i()
-    step = pl.program_id(0)
-
-    @pl.when(step == 0)
-    def _():
-        for kind, value in enumerate(scales(sq_ref[...])):
-            scale_ref[kind] = jnp.full((8, 128), value, F32)
-
-    scale = [scale_ref[kind, 0:1, 0:1] for kind in range(2)]
-    m = m_ref[...].reshape(256, W)
-    for kind, out in enumerate((ic_out, gc_out)):
-        basis = f_ref[kind].reshape(256, RANK)
+    order = (HERE, 2, 4, 1, 5, 0, 6, 7)
+    row = [lax.rem(z + k + 8 - HERE, 8) for k in range(8)]
+    loads = [pltpu.make_async_copy(sq_hbm, sqv, s_n.at[0]), pltpu.make_async_copy(n_hbm, nv, s_n.at[1])]
+    for cp in loads:
+        cp.start()
+    fs = [pltpu.make_async_copy(f_hbm.at[:, row[k]], fv.at[k], s_f.at[k]) for k in range(8)]
+    ms = [pltpu.make_async_copy(m_hbm.at[k], mv.at[k], s_m.at[k]) for k in range(8)]
+    for k in order:
+        fs[k].start()
+        ms[k].start()
+
+    for kind, (f_old, s_old, f_new, s_new) in enumerate(
+        ((i1_ref, i2_ref, i1_out, i2_out), (g1_ref, g2_ref, g1_out, g2_out))
+    ):
         for h in range(2):
-            normed = n_ref[2 * kind + h].reshape(RANK, 256)
-            full = jnp.dot(basis, normed, preferred_element_type=F32)
-            col = 256 * h
-            old = m[:, kind * 512 + col : kind * 512 + col + 256].astype(F32)
-            out[:, col : col + 256] = (old - 0.05 * (full * scale[kind])).astype(BF)
-
-    @pl.when(step == z)
-    def _():
-        for kind, (old, new, upd) in enumerate(((im_ref, im_out, iu_out), (gm_ref, gm_out, gu_out))):
-            basis = f_ref[kind, 0, y].reshape(64, RANK)
+            low = low_ref[2 * kind + h]
+            cols = slice(256 * h, 256 * h + 256)
+            f_new[:, cols] = 0.8 * f_old[:, cols] + 0.2 * low
+            s_new[:, cols] = 0.95 * s_old[:, cols] + 0.05 * low * low
+
+    loads[0].wait()
+    scale = []
+    for kind in range(2):
+        square = jnp.sum(sqv[0, kind] + sqv[1, kind], axis=(0, 1), keepdims=True)
+        scale.append(lax.rsqrt(square / (D * W) + 0.1))
+    loads[1].wait()
+    outs = []
+    for k in order:
+        fs[k].wait()
+        if k == HERE:
+            for kind, (old, new, upd) in enumerate(((im_ref, im_out, iu_out), (gm_ref, gm_out, gu_out))):
+                basis = fv[k, kind, y].reshape(64, RANK)
+                for h in range(2):
+                    normed = nv[2 * kind + h].reshape(RANK, 256)
+                    cols = slice(256 * h, 256 * h + 256)
+                    u = jnp.dot(basis, normed, preferred_element_type=F32) * scale[kind]
+                    upd[:, cols] = u
+                    new[:, cols] = old[:, cols] - 0.05 * u
+        ms[k].wait()
+        for kind, out in enumerate((ic_out, gc_out)):
+            basis = fv[k, kind].reshape(256, RANK)
             for h in range(2):
-                normed = n_ref[2 * kind + h].reshape(RANK, 256)
-                cols = slice(256 * h, 256 * h + 256)
-                u = jnp.dot(basis, normed, preferred_element_type=F32) * scale[kind]
-                upd[:, cols] = u
-                new[:, cols] = old[:, cols] - 0.05 * u
-
-    @pl.when(step == 0)
-    def _():
-        for kind, (f_old, s_old, f_new, s_new) in enumerate(
-            ((i1_ref, i2_ref, i1_out, i2_out), (g1_ref, g2_ref, g1_out, g2_out))
-        ):
-            for h in range(2):
-                low = low_ref[2 * kind + h]
-                cols = slice(256 * h, 256 * h + 256)
-                f_new[:, cols] = 0.8 * f_old[:, cols] + 0.2 * low
-                s_new[:, cols] = 0.95 * s_old[:, cols] + 0.05 * low * low
+                normed = nv[2 * kind + h].reshape(RANK, 256)
+                full = jnp.dot(basis, normed, preferred_element_type=F32)
+                col = kind * 512 + 256 * h
+                old = mv[k, :, :, col : col + 256].reshape(256, 256).astype(F32)
+                cv[k, kind, :, 256 * h : 256 * h + 256] = (old - 0.05 * (full * scale[kind])).astype(BF)
+            rows = pl.ds(pl.multiple_of(row[k] * 256, 256), 256)
+            cp = pltpu.make_async_copy(cv.at[k, kind], out.at[rows, :], s_c.at[k, kind])
+            cp.start()
+            outs.append(cp)
+    for cp in outs:
+        cp.wait()
 
 
 def written(f, n, m, sq, low, im, gm, i1, i2, g1, g2):
-    def fixed(shape):
-        return pl.BlockSpec(shape, lambda i: (0,) * len(shape))
-
-    own, mo = fixed((64, 512)), fixed((8, 512))
+    sem, whole, kept = pltpu.SemaphoreType.DMA, pl.BlockSpec(memory_space=pltpu.VMEM), pl.BlockSpec(memory_space=ANY)
     return pl.pallas_call(
         write_kernel,
         name="write",
-        grid=(NZ,),
         out_shape=(
             *[jax.ShapeDtypeStruct((64, 512), F32)] * 4,
             *[jax.ShapeDtypeStruct((8, 512), F32)] * 4,
             *[jax.ShapeDtypeStruct((D, 512), BF)] * 2,
         ),
-        in_specs=[
-            pl.BlockSpec((2, 1, NY, NX, 16, RANK), lambda i: (0, i, 0, 0, 0, 0)),
-            fixed((NX, NY, 64, 256)),
-            pl.BlockSpec((1, NY, 64, W), lambda i: (i, 0, 0, 0)),
-            fixed((2, 2, 8, 128)),
-            fixed((NX, 8, 256)),
-            own, own, mo, mo, mo, mo,
+        in_specs=[kept] * 4 + [whole] * 7,
+        out_specs=[whole] * 8 + [kept] * 2,
+        scratch_shapes=[
+            pltpu.VMEM((8, 2, NY, NX, 16, RANK), BF),
+            pltpu.VMEM((NX, NY, 64, 256), BF),
+            pltpu.VMEM((8, NY, 64, W), BF),
+            pltpu.VMEM((2, 2, 8, 128), F32),
+            pltpu.VMEM((8, 2, 256, 512), BF),
+            sem((8,)),
+            sem((2,)),
+            sem((8,)),
+            sem((8, 2)),
         ],
-        out_specs=[own] * 4 + [mo] * 4 + [pl.BlockSpec((256, 512), lambda i: (i, 0))] * 2,
-        scratch_shapes=[pltpu.VMEM((2, 8, 128), F32)],
-        compiler_params=pltpu.CompilerParams(
-            dimension_semantics=("arbitrary",), vmem_limit_bytes=VMEM
-        ),
+        compiler_params=pltpu.CompilerParams(vmem_limit_bytes=VMEM),
     )(f, n, m, sq, low, im, gm, i1, i2, g1, g2)
 
 

time: 78.2 us -> 72.4 us (0.926)
  Pallas kernels: 77.3 us -> 71.7 us
    pallas_call x1, Pallas kernels: 68.3 us -> 63.4 us  [gathered(): pl.pallas_call(move_kernel, name='move', out_shape=(jax.ShapeDtypeStruct(...]
where the time goes in v3:
time: 72.4 us; the launch traced here: 72.3 us
  Pallas kernels  71.7 us (99%)
    pallas_call x1, Pallas kernels, gathered(): pl.pallas_call(move_kernel, name='move', out_shape=(jax.ShapeDtypeStruct(...  63.4 us
    pallas_call x1, Pallas kernels, written(): pl.pallas_call(write_kernel, name='write', out_shape=(*[jax.ShapeDtypeStr...  8.28 us

profile of v3, /device:TPU:1, one launch (start us, length us, event | category | flops | bytes accessed | tf_op | source)
XLA Modules:
  0.0 72.3 jit_solution(13278870270222587019)
XLA Ops:
  0.6 63.4 %move.1 = (bf16[8,4,64,1024]{3,2,1,0:T(8,128)(2,1)}, bf16[2,8,4,4,16,256]{5,4,3,2,1,0:T(8,128)(2,1)}, bf16[4,4,64,256]{3,2,1,0:T(8,128)(2,1)}, f32[4,8,256]{2,1,0:T(8,128)}, f32[2,2,8,128]{3,2,1,0:T(8,128)}) custom-call(bf16[1024,2048]{1,0:T(8,128)(2,1)} %x_hbm.1, bf16[1024,512]{1,0:T(8,128)(2,1)} %ci_hbm.1, bf16[1024,512]{1,0:T(8,128)(2,1)} %cg_hbm.1, ...), custom_call_target="tpu_custom_call" | custom-call | flops 6000000000 | bytes 16777216 | tf_op jit(solution)/shard_map/move/pallas_call | solution.py:390
  64.1 8.3 %write.1 = (f32[64,512]{1,0:T(8,128)}, f32[64,512]{1,0:T(8,128)}, f32[64,512]{1,0:T(8,128)}, f32[64,512]{1,0:T(8,128)}, f32[8,512]{1,0:T(8,128)}, /*index=5*/f32...) custom-call(bf16[2,8,4,4,16,256]{5,4,3,2,1,0:T(8,128)(2,1)} %get-tuple-e, ...), custom_call_target="tpu_custom_call" | custom-call | tf_op jit(solution)/shard_map/write/pallas_call | solution.py:500

commit v4 on v3

v4 whole, which is shorter than its diff:
```python
import jax
import jax.numpy as jnp
from jax import lax
from jax.experimental import pallas as pl
from jax.experimental.pallas import tpu as pltpu
from jax.sharding import PartitionSpec as P

D = 2048
W = 1024
RANK = 256
NX, NY, NZ = 4, 4, 8
YZ_COLS, YZ0, YZ1 = pl.ds(0, 512), pl.ds(0, 256), pl.ds(256, 256)
ZY_COLS, ZYX_COLS, Z_COLS = pl.ds(512, 128), pl.ds(640, 384), pl.ds(512, 512)
HERE = 3
NEAR, BELOW, ABOVE = pl.ds(2, 3), pl.ds(0, 2), pl.ds(5, 3)
BF = jnp.bfloat16
F32 = jnp.float32
VMEM = 67_043_328
ANY = pl.ANY

XY = sorted(
    [(a, b) for a in range(4) for b in range(4) if (a, b) != (0, 0)],
    key=lambda o: -(min(o[0], 4 - o[0]) + min(o[1], 4 - o[1])),
)
ZD = sorted(range(1, 8), key=lambda d: -min(d, 8 - d))


def where_am_i():
    fs, x, c = lax.axis_index("fs"), lax.axis_index("rep"), lax.axis_index("tp")
    return x, lax.rem(fs, 4), lax.div(fs, 4), c


GROUPS = ("fz", "mo", "by", "ra", "rb", "rc", "fab", "fcd", "ft", "rs", "quarter", "whole", "across", "zs", "lo", "ag", "sq")
SEM = {name: k for k, name in enumerate(GROUPS)}


def take(region, sem):
    pltpu.make_async_copy(region, region, sem).wait()


def remote(src, dst, ss, rs, dev):
    return pltpu.make_async_remote_copy(
        src_ref=src,
        dst_ref=dst,
        send_sem=ss,
        recv_sem=rs,
        device_id=dev,
        device_id_type=pl.DeviceIdType.MESH,
    )


def move_kernel(
    x_hbm, ci_hbm, cg_hbm, im_hbm, gm_hbm, if_hbm, gf_hbm, i1_hbm, i2_hbm, g1_hbm, g2_hbm,
    m_out, f_out, n_out, low_out, sq_out,
    xv, cot, cot_t, grad_t, fac, fsh, fall, mast, msh, mom_in, mom_own, mom,
    part, rsb, zb, nb, lowb, sqb,
    s_loc, sent, got, ring_got, pair_got, land_got, leg_got,
):
    x, y, z, c = where_am_i()

    def at(dx, dy, dz, dc=0):
        return {
            "fs": lax.rem(z + dz, 8) * 4 + lax.rem(y + dy, 4),
            "rep": lax.rem(x + dx, 4),
            "tp": lax.rem(c + dc, 2),
        }

    def s_of(name):
        return sent.at[SEM[name]]

    def g_of(name):
        return got.at[SEM[name]]

    @pl.when(c == 0)
    def _():
        pltpu.make_async_copy(if_hbm, fac, s_loc.at[0]).start()

    @pl.when(c == 1)
    def _():
        pltpu.make_async_copy(gf_hbm, fac, s_loc.at[0]).start()

    moms = [
        pltpu.make_async_copy(r, mom_in.at[k], s_loc.at[1 + k])
        for k, r in enumerate((i1_hbm, g1_hbm, i2_hbm, g2_hbm))
    ]
    masters = [
        pltpu.make_async_copy(r, mast.at[k], s_loc.at[5 + k]) for k, r in enumerate((im_hbm, gm_hbm))
    ]
    cots = [
        pltpu.make_async_copy(r, cot.at[k], s_loc.at[7 + k]) for k, r in enumerate((ci_hbm, cg_hbm))
    ]
    load_x = pltpu.make_async_copy(x_hbm, xv, s_loc.at[9])
    for cp in (*moms, *masters, *cots, load_x):
        cp.start()

    barrier = pltpu.get_barrier_semaphore()
    peers = [at(a, b, 0) for a, b in XY] + [at(0, 0, d) for d in ZD] + [at(0, 0, 0, 1)]
    for p in peers:
        pl.semaphore_signal(barrier, inc=1, device_id=p, device_id_type=pl.DeviceIdType.MESH)

    pltpu.make_async_copy(if_hbm, fac, s_loc.at[0]).wait()
    new = lax.broadcasted_iota(jnp.int32, (RANK, RANK), 1)
    old = lax.broadcasted_iota(jnp.int32, (RANK, RANK), 0)
    ny, nz, ni = lax.shift_right_logical(new, 6), (lax.shift_right_logical(new, 3) & 7), new & 7
    perm = jnp.where(old == (nz * 4 + ny) * 8 + ni, 1.0, 0.0).astype(BF)
    shard = jnp.dot(fac[...], perm, preferred_element_type=F32).astype(BF)
    fsh[...] = shard.reshape(4, 16, RANK)
    fall[c, z, y, x] = fsh[x]

    for cp in moms:
        cp.wait()
    for q in range(4):
        kind, col = q // 2, (q % 2) * 256
        mom_own[q, 0] = mom_in[kind, :, col : col + 256]
        mom_own[q, 1] = mom_in[2 + kind, :, col : col + 256]
    mom[z] = mom_own[x]

    for cp in masters:
        cp.wait()
    msh[:, :512] = mast[0].astype(BF)
    msh[:, 512:] = mast[1].astype(BF)
    keep_m = pltpu.make_async_copy(msh, m_out.at[HERE, y], s_loc.at[10])
    keep_m.start()

    pl.semaphore_wait(barrier, len(peers))

    fz = [
        remote(fsh.at[x], fall.at[c, z, y, x], s_of("fz"), g_of("fz"), at(0, 0, d))
        for k, d in enumerate(ZD)
    ]
    mo = [remote(mom_own.at[x], mom.at[z], s_of("mo"), g_of("mo"), at(0, 0, d)) for k, d in enumerate(ZD)]
    by = [
        remote(msh.at[:, YZ_COLS], m_out.at[HERE, y, :, YZ_COLS], s_of("by"), g_of("by"), at(0, b, 0))
        for k, b in enumerate((2, 1, 3))
    ]

    def ring(block, n):
        ss, rs = s_of(("ra", "rb", "rc")[n]), ring_got.at[n]
        hops = []
        for h in range(4):
            lower, upper = (pl.ds(0, 32), pl.ds(32, 32)) if h == 3 else (pl.ds(0, 64),) * 2
            up = (block(HERE - h, lower), block(HERE - h - 1 if h < 3 else HERE + 4, lower))
            down = (block(HERE + h, upper), block(HERE + h + 1, upper))
            hops.append(
                (
                    remote(*up, ss, rs.at[h], at(0, 0, 1)),
                    remote(*down, ss, rs.at[h], at(0, 0, 7)),
                )
            )
        return hops

    ra = ring(lambda k, rows: m_out.at[k, y, rows, Z_COLS], 0)
    rb = ring(lambda k, rows: m_out.at[k, :, rows, YZ0], 1)
    rc = ring(lambda k, rows: m_out.at[k, :, rows, YZ1], 2)
    every = pl.ds(0, 64)

    def ring_blocks(n, count):
        if n == 0:
            return m_out.at[pl.ds(0, count), y, :, Z_COLS]
        return m_out.at[pl.ds(0, count), :, :, (YZ0, YZ1)[n - 1]]

    def landed(n, h):
        take(ring_blocks(n, 2 if h < 3 else 1), ring_got.at[n, h])

    def hop(n, h):
        if h:
            landed(n, h - 1)
        for cp in (ra, rb, rc)[n][h]:
            cp.start()

    for cp in (*fz, *by):
        cp.start()
    keep_m.wait()
    hop(0, 0)

    rows16 = pl.ds(pl.multiple_of(x * 16, 16), 16)
    part_of = {"near": NEAR, "below": BELOW, "above": ABOVE}

    def along_y(group, rows, cols, name, rsem):
        block = m_out.at[part_of[group], y, rows, cols]
        return [
            remote(block, block, s_of(name), rsem, at(0, b, 0))
            for b in (2, 1, 3)
        ]

    def along_x(group):
        out = []
        for a in (2, 1, 3):
            for j in range(3):
                block = m_out.at[part_of[group], lax.rem(y + 1 + j, 4), rows16, ZYX_COLS]
                out.append(remote(block, block, s_of("across"), g_of("across"), at(a, 0, 0)))
        return out

    groups = ("near", "below", "above")
    quarters = {g: along_y(g, rows16, ZYX_COLS, "quarter", leg_got.at[k]) for k, g in enumerate(groups)}
    wholes = {g: along_y(g, every, ZY_COLS, "whole", g_of("whole")) for g in groups}
    acrosses = {g: along_x(g) for g in groups}

    def start(*lists):
        for cps in lists:
            for cp in cps:
                cp.start()

    def quarters_arrive(k):
        take(m_out.at[pl.ds(0, (3, 2, 3)[k]), pl.ds(0, 3), pl.ds(0, 16), ZYX_COLS], leg_got.at[k])

    for cp in cots:
        cp.wait()
    for k in range(2):
        cot_t[k * 512 : (k + 1) * 512, :] = cot[k].T
    load_x.wait()

    def grad_step(i, _):
        cols = pl.ds(pl.multiple_of(i * 256, 256), 256)
        grad_t[:, cols] = jnp.dot(cot_t[...], xv[:, cols], preferred_element_type=F32).astype(BF)
        return 0

    lax.fori_loop(0, 2, grad_step, 0)

    take(fall.at[c, pl.ds(0, 7), 0, 0], g_of("fz"))
    def piece(half, xs, ys):
        return fall.at[c, pl.ds(4 * half, 4), ys, xs]

    def send_piece(half, xs, ys, ss, rs, dev):
        block = piece(half, xs, ys)
        return remote(block, block, ss, rs, dev)

    def back(p, d):
        return lax.rem(p + 4 - d, 4)

    near = (1, 3, 2)
    fa = [send_piece(0, x, y, s_of("fab"), pair_got.at[k], at(0, b, 0)) for k, b in enumerate(near)]
    fb = [send_piece(1, x, y, s_of("fab"), pair_got.at[k], at(a, 0, 0)) for k, a in enumerate(near)]
    ysrc = [y] + [back(y, b) for b in near]
    xsrc = [x] + [back(x, a) for a in near]
    fc = [
        [send_piece(0, x, ys, s_of("fcd"), land_got.at[i], at(a, 0, 0)) for a in near]
        for i, ys in enumerate(ysrc)
    ]
    fd = [
        [send_piece(1, xs, y, s_of("fcd"), land_got.at[i], at(0, b, 0)) for b in near]
        for i, xs in enumerate(xsrc)
    ]

    def to_partner(half, xs, ys):
        send_piece(half, xs, ys, s_of("ft"), g_of("ft"), at(0, 0, 0, 1)).start()

    start(fa, fb, fc[0], fd[0])
    to_partner(0, x, y)
    to_partner(1, x, y)

    lax.fori_loop(2, 4, grad_step, 0)
    hop(0, 1)
    start(quarters["near"])
    take(m_out.at[0, pl.ds(0, 3), :, YZ_COLS], g_of("by"))
    hop(1, 0)

    def relay(k):
        take(fall.at[c, :, 0, 0], pair_got.at[k])
        start(fc[1 + k], fd[1 + k])
        to_partner(0, x, ysrc[1 + k])
        to_partner(1, xsrc[1 + k], y)

    relay(0)
    relay(1)
    lax.fori_loop(4, 5, grad_step, 0)
    relay(2)
    hop(0, 2)
    hop(2, 0)
    lax.fori_loop(5, 7, grad_step, 0)

    def land(i):
        take(fall.at[c, :, pl.ds(0, 3), 0], land_got.at[i])
        for k in range(3):
            to_partner(0, xsrc[1 + k], ysrc[i])
            to_partner(1, xsrc[i], ysrc[1 + k])

    land(0)
    quarters_arrive(0)
    start(acrosses["near"], wholes["near"])
    lax.fori_loop(7, 8, grad_step, 0)
    land(1)
    land(2)
    hop(0, 3)
    land(3)
    hop(1, 1)
    hop(2, 1)
    start(mo)
    take(fall.at[1 - c], g_of("ft"))

    for dx in (2, 1, 3, 0):
        q = lax.rem(x + dx, 4)
        kind = lax.div(q, 2)
        basis = fall[kind].reshape(D, RANK)
        rows = pl.ds(pl.multiple_of(q * 256, 256), 256)
        low_t = jnp.dot(grad_t[rows, :], basis, preferred_element_type=F32)
        part[q] = low_t.T.astype(BF).reshape(4, 64, 256)
        for k, (a, b) in enumerate(XY):
            if a == dx:
                remote(part.at[q, lax.rem(y + b, 4)], rsb.at[k], s_of("rs"), g_of("rs"), at(a, b, 0)).start()

    landed(0, 3)
    start(quarters["below"], quarters["above"])
    hop(1, 2)
    hop(2, 2)

    keep_f = pltpu.make_async_copy(fall, f_out, s_loc.at[11])
    keep_f.start()

    grams = []
    for kind in range(2):
        basis = fall[kind].reshape(D, RANK)
        g = lax.dot_general(basis, basis, (((0,), (0,)), ((), ())), preferred_element_type=F32)
        hi = g.astype(BF)
        grams.append((hi, (g - hi.astype(F32)).astype(BF)))

    start(wholes["below"], wholes["above"])
    total = part[x, y].astype(F32)
    take(rsb, g_of("rs"))
    for k in range(15):
        total = total + rsb[k].astype(F32)
    zb[z] = total.astype(BF)
    zs = [remote(zb.at[z], zb.at[z], s_of("zs"), g_of("zs"), at(0, 0, d)) for k, d in enumerate(ZD)]
    for cp in zs:
        cp.start()
    hop(1, 3)
    quarters_arrive(2)
    start(acrosses["above"])
    hop(2, 3)
    quarters_arrive(1)
    take(mom.at[pl.ds(0, 7)], g_of("mo"))
    first = mom[:, 0].reshape(64, 256)
    second = mom[:, 1].reshape(64, 256)
    take(zb.at[pl.ds(0, 7)], g_of("zs"))
    low = zb[0].astype(F32)
    for k in range(1, 8):
        low = low + zb[k].astype(F32)
    first_new = 0.8 * first + 0.2 * low
    second_new = 0.95 * second + 0.05 * low * low
    nb[x, y] = (first_new / jnp.sqrt(second_new)).astype(BF)
    ag = [
        remote(nb.at[x, y], nb.at[x, y], s_of("ag"), g_of("ag"), at(a, b, 0))
        for k, (a, b) in enumerate(XY)
    ]
    for cp in ag:
        cp.start()

    part_low = low.reshape(8, 8, 256)
    mine = jnp.zeros((8, 256), F32)
    for k in range(8):
        mine = jnp.where(z == k, part_low[k], mine)
    lowb[x] = mine
    lo = [remote(lowb.at[x], lowb.at[x], s_of("lo"), g_of("lo"), at(a, 0, 0)) for a in (2, 1, 3)]
    for cp in lo:
        cp.start()
    start(acrosses["below"])

    take(rsb, g_of("ag"))
    keep_n = pltpu.make_async_copy(nb, n_out, s_loc.at[12])
    keep_n.start()
    for kind in range(2):
        acc = jnp.zeros((8, 128), F32)
        for q in (2 * kind, 2 * kind + 1):
            normed = nb[q].reshape(RANK, 256)
            t = jnp.dot(grams[kind][0], normed, preferred_element_type=F32)
            t = t + jnp.dot(grams[kind][1], normed, preferred_element_type=F32)
            s = jnp.sum((t * normed.astype(F32)).reshape(32, 8, 256), axis=0)
            acc = acc + s[:, :128] + s[:, 128:]
        sqb[c, kind] = acc
    sq = remote(sqb.at[c], sqb.at[c], s_of("sq"), g_of("sq"), at(0, 0, 0, 1))
    sq.start()
    take(lowb.at[pl.ds(0, 3)], g_of("lo"))
    keep_low = pltpu.make_async_copy(lowb, low_out, s_loc.at[13])
    keep_low.start()
    take(sqb.at[0], g_of("sq"))
    keep_sq = pltpu.make_async_copy(sqb, sq_out, s_loc.at[14])
    keep_sq.start()
    landed(1, 3)
    landed(2, 3)
    spread = {
        "whole": m_out.at[:, pl.ds(0, 3), :, ZY_COLS],
        "across": m_out.at[:, pl.ds(0, 3), pl.ds(0, 48), ZYX_COLS],
    }
    for name, region in spread.items():
        take(region, g_of(name))
    gone = {
        "fz": fall.at[0, pl.ds(0, 7), 0, 0],
        "mo": mom.at[pl.ds(0, 7)],
        "by": m_out.at[0, pl.ds(0, 3), :, YZ_COLS],
        "ra": ring_blocks(0, 7),
        "rb": ring_blocks(1, 7),
        "rc": ring_blocks(2, 7),
        "fab": fall.at[0, :, pl.ds(0, 3), 0],
        "fcd": fall.at[0, :, :, pl.ds(0, 3)],
        "ft": fall.at[0],
        "rs": rsb,
        "quarter": m_out.at[:, pl.ds(0, 3), pl.ds(0, 16), ZYX_COLS],
        "zs": zb.at[pl.ds(0, 7)],
        "ag": rsb,
        "lo": lowb.at[pl.ds(0, 3)],
        "sq": sqb.at[0],
        **spread,
    }
    for name in GROUPS:
        take(gone[name], s_of(name))
    for cp in (keep_f, keep_n, keep_low, keep_sq):
        cp.wait()


def gathered(x, ci, cg, im, gm, inf, gf, i1, i2, g1, g2):
    sem = pltpu.SemaphoreType.DMA
    return pl.pallas_call(
        move_kernel,
        name="move",
        out_shape=(
            jax.ShapeDtypeStruct((NZ, NY, 64, W), BF),
            jax.ShapeDtypeStruct((2, NZ, NY, NX, 16, RANK), BF),
            jax.ShapeDtypeStruct((NX, NY, 64, 256), BF),
            jax.ShapeDtypeStruct((NX, 8, 256), F32),
            jax.ShapeDtypeStruct((2, 2, 8, 128), F32),
        ),
        in_specs=[pl.BlockSpec(memory_space=ANY)] * 11,
        out_specs=[pl.BlockSpec(memory_space=ANY)] * 5,
        scratch_shapes=[
            pltpu.VMEM((1024, D), BF),
            pltpu.VMEM((2, 1024, 512), BF),
            pltpu.VMEM((1024, 1024), BF),
            pltpu.VMEM((1024, D), BF),
            pltpu.VMEM((64, RANK), BF),
            pltpu.VMEM((4, 16, RANK), BF),
            pltpu.VMEM((2, NZ, NY, NX, 16, RANK), BF),
            pltpu.VMEM((2, 64, 512), F32),
            pltpu.VMEM((64, W), BF),
            pltpu.VMEM((4, 8, 512), F32),
            pltpu.VMEM((4, 2, 8, 256), F32),
            pltpu.VMEM((NZ, 2, 8, 256), F32),
            pltpu.VMEM((NX, NY, 64, 256), BF),
            pltpu.VMEM((15, 64, 256), BF),
            pltpu.VMEM((NZ, 64, 256), BF),
            pltpu.VMEM((NX, NY, 64, 256), BF),
            pltpu.VMEM((NX, 8, 256), F32),
            pltpu.VMEM((2, 2, 8, 128), F32),
            sem((15,)),
            sem((len(GROUPS),)),
            sem((len(GROUPS),)),
            sem((3, 4)),
            sem((3,)),
            sem((4,)),
            sem((3,)),
        ],
        compiler_params=pltpu.CompilerParams(
            collective_id=0, has_side_effects=True, vmem_limit_bytes=VMEM
        ),
        cost_estimate=pl.CostEstimate(flops=6 * 10**9, bytes_accessed=16 * 2**20, transcendentals=0),
    )(x, ci, cg, im, gm, inf, gf, i1, i2, g1, g2)


def write_kernel(
    f_hbm, n_hbm, m_hbm, sq_hbm, low_hbm, im_hbm, gm_hbm, i1_hbm, i2_hbm, g1_hbm, g2_hbm,
    im_out, gm_out, iu_out, gu_out, i1_out, i2_out, g1_out, g2_out, ic_out, gc_out,
    fv, nv, mv, sqv, lowv, old_v, new_v, upd_v, mom_v, mom_new, cv, s_f, s_m, s_in, s_c, s_out,
):
    _, y, z, _ = where_am_i()
    order = (HERE, 2, 4, 1, 5, 0, 6, 7)
    row = [lax.rem(z + k + 8 - HERE, 8) for k in range(8)]
    small = [
        (sq_hbm, sqv), (n_hbm, nv), (im_hbm, old_v.at[0]), (gm_hbm, old_v.at[1]), (low_hbm, lowv),
        *[(r, mom_v.at[k]) for k, r in enumerate((i1_hbm, i2_hbm, g1_hbm, g2_hbm))],
    ]
    small = [pltpu.make_async_copy(src, dst, s_in.at[k]) for k, (src, dst) in enumerate(small)]
    fs = [pltpu.make_async_copy(f_hbm.at[:, row[k]], fv.at[k], s_f.at[k]) for k in range(8)]
    ms = [pltpu.make_async_copy(m_hbm.at[k], mv.at[k], s_m.at[k]) for k in range(8)]
    small[0].start()
    small[1].start()
    fs[HERE].start()
    ms[HERE].start()
    for cp in small[2:]:
        cp.start()
    outs = []

    def put(src, dst, sem):
        cp = pltpu.make_async_copy(src, dst, sem)
        cp.start()
        outs.append(cp)

    small[0].wait()
    for k in order[1:]:
        fs[k].start()
        ms[k].start()
    scale = []
    for kind in range(2):
        square = jnp.sum(sqv[0, kind] + sqv[1, kind], axis=(0, 1), keepdims=True)
        scale.append(lax.rsqrt(square / (D * W) + 0.1))
    small[1].wait()
    for at, k in enumerate(order):
        fs[k].wait()
        ms[k].wait()
        for kind, out in enumerate((ic_out, gc_out)):
            basis = fv[k, kind].reshape(256, RANK)
            for h in range(2):
                normed = nv[2 * kind + h].reshape(RANK, 256)
                full = jnp.dot(basis, normed, preferred_element_type=F32)
                col = kind * 512 + 256 * h
                old = mv[k, :, :, col : col + 256].reshape(256, 256).astype(F32)
                cv[k, kind, :, 256 * h : 256 * h + 256] = (old - 0.05 * (full * scale[kind])).astype(BF)
            rows = pl.ds(pl.multiple_of(row[k] * 256, 256), 256)
            put(cv.at[k, kind], out.at[rows, :], s_c.at[k, kind])
        if at == 0:
            for cp in small[2:]:
                cp.wait()
            for kind, (new_out, upd_out) in enumerate(((im_out, iu_out), (gm_out, gu_out))):
                basis = fv[k, kind, y].reshape(64, RANK)
                for h in range(2):
                    normed = nv[2 * kind + h].reshape(RANK, 256)
                    cols = slice(256 * h, 256 * h + 256)
                    u = jnp.dot(basis, normed, preferred_element_type=F32) * scale[kind]
                    upd_v[kind, :, cols] = u
                    new_v[kind, :, cols] = old_v[kind, :, cols] - 0.05 * u
                put(upd_v.at[kind], upd_out, s_out.at[2 * kind])
                put(new_v.at[kind], new_out, s_out.at[2 * kind + 1])
            for kind, (first_out, second_out) in enumerate(((i1_out, i2_out), (g1_out, g2_out))):
                for h in range(2):
                    low = lowv[2 * kind + h]
                    cols = slice(256 * h, 256 * h + 256)
                    mom_new[2 * kind, :, cols] = 0.8 * mom_v[2 * kind, :, cols] + 0.2 * low
                    mom_new[2 * kind + 1, :, cols] = 0.95 * mom_v[2 * kind + 1, :, cols] + 0.05 * low * low
                put(mom_new.at[2 * kind], first_out, s_out.at[4 + 2 * kind])
                put(mom_new.at[2 * kind + 1], second_out, s_out.at[5 + 2 * kind])
    for cp in outs:
        cp.wait()


def written(f, n, m, sq, low, im, gm, i1, i2, g1, g2):
    sem, kept = pltpu.SemaphoreType.DMA, pl.BlockSpec(memory_space=ANY)
    return pl.pallas_call(
        write_kernel,
        name="write",
        out_shape=(
            *[jax.ShapeDtypeStruct((64, 512), F32)] * 4,
            *[jax.ShapeDtypeStruct((8, 512), F32)] * 4,
            *[jax.ShapeDtypeStruct((D, 512), BF)] * 2,
        ),
        in_specs=[kept] * 11,
        out_specs=[kept] * 10,
        scratch_shapes=[
            pltpu.VMEM((8, 2, NY, NX, 16, RANK), BF),
            pltpu.VMEM((NX, NY, 64, 256), BF),
            pltpu.VMEM((8, NY, 64, W), BF),
            pltpu.VMEM((2, 2, 8, 128), F32),
            pltpu.VMEM((NX, 8, 256), F32),
            *[pltpu.VMEM((2, 64, 512), F32)] * 3,
            *[pltpu.VMEM((4, 8, 512), F32)] * 2,
            pltpu.VMEM((8, 2, 256, 512), BF),
            *[sem((n,)) for n in (8, 8, 9)],
            sem((8, 2)),
            sem((8,)),
        ],
        compiler_params=pltpu.CompilerParams(vmem_limit_bytes=VMEM),
    )(f, n, m, sq, low, im, gm, i1, i2, g1, g2)


def on_device(x, ci, cg, im, gm, inf, gf, i1, i2, g1, g2):
    m, f, n, low, sq = gathered(x, ci, cg, im, gm, inf, gf, i1, i2, g1, g2)
    out = written(f, n, m, sq, low, im, gm, i1, i2, g1, g2)
    return tuple(out)


def solution(mesh):
    tokens, rows, moments = P(("fs", "rep"), "tp"), P("fs", "tp"), P("fs", "tp")
    return jax.shard_map(
        on_device,
        mesh=mesh,
        in_specs=(
            P(("fs", "rep"), None), tokens, tokens, rows, rows, P("fs", None), P("fs", None),
            moments, moments, moments, moments,
        ),
        out_specs=(rows,) * 4 + (moments,) * 4 + (P(None, "tp"),) * 2,
        check_vma=False,
    )
```

time: 72.4 us -> 66.1 us (0.913)
  Pallas kernels: 71.7 us -> 65.3 us
    pallas_call x1, Pallas kernels: 63.4 us -> 59.3 us  [gathered(): pl.pallas_call(move_kernel, name='move', out_shape=(jax.ShapeDtypeStruct(...]
    pallas_call x1, Pallas kernels: 8.28 us -> 5.98 us  [written(): pl.pallas_call(write_kernel, name='write', out_shape=(*[jax.ShapeDtypeStr...]
where the time goes in v4:
time: 66.1 us; the launch traced here: 65.9 us
  Pallas kernels  65.3 us (99%)
    pallas_call x1, Pallas kernels, gathered(): pl.pallas_call(move_kernel, name='move', out_shape=(jax.ShapeDtypeStruct(...  59.3 us
    pallas_call x1, Pallas kernels, written(): pl.pallas_call(write_kernel, name='write', out_shape=(*[jax.ShapeDtypeStr...  5.98 us

profile of v4, /device:TPU:1, one launch (start us, length us, event | category | flops | bytes accessed | tf_op | source)
XLA Modules:
  0.0 65.9 jit_solution(9443196289719157312)
XLA Ops:
  0.6 59.3 %move.1 = (bf16[8,4,64,1024]{3,2,1,0:T(8,128)(2,1)}, bf16[2,8,4,4,16,256]{5,4,3,2,1,0:T(8,128)(2,1)}, bf16[4,4,64,256]{3,2,1,0:T(8,128)(2,1)}, f32[4,8,256]{2,1,0:T(8,128)}, f32[2,2,8,128]{3,2,1,0:T(8,128)}) custom-call(bf16[1024,2048]{1,0:T(8,128)(2,1)} %x_hbm.1, bf16[1024,512]{1,0:T(8,128)(2,1)} %ci_hbm.1, bf16[1024,512]{1,0:T(8,128)(2,1)} %cg_hbm.1, ...), custom_call_target="tpu_custom_call" | custom-call | flops 6000000000 | bytes 16777216 | tf_op jit(solution)/shard_map/move/pallas_call | solution.py:412
  60.0 6.0 %write.1 = (f32[64,512]{1,0:T(8,128)}, f32[64,512]{1,0:T(8,128)}, f32[64,512]{1,0:T(8,128)}, f32[64,512]{1,0:T(8,128)}, f32[8,512]{1,0:T(8,128)}, /*index=5*/f32...) custom-call(bf16[2,8,4,4,16,256]{5,4,3,2,1,0:T(8,128)(2,1)} %get-tuple-e, ...), custom_call_target="tpu_custom_call" | custom-call | tf_op jit(solution)/shard_map/write/pallas_call | solution.py:535

commit v5 on v4

--- a/solution.py
+++ b/solution.py
@@ -1,3 +1,5 @@
+import functools
+
 import jax
 import jax.numpy as jnp
 from jax import lax
@@ -9,8 +11,8 @@
 W = 1024
 RANK = 256
 NX, NY, NZ = 4, 4, 8
-YZ_COLS, YZ0, YZ1 = pl.ds(0, 512), pl.ds(0, 256), pl.ds(256, 256)
-ZY_COLS, ZYX_COLS, Z_COLS = pl.ds(512, 128), pl.ds(640, 384), pl.ds(512, 512)
+YZ_COLS, YZ0, YZ1 = pl.ds(0, 384), pl.ds(0, 256), pl.ds(256, 128)
+ZY_COLS, ZYX_COLS, Z_COLS = pl.ds(384, 256), pl.ds(640, 384), pl.ds(384, 640)
 HERE = 3
 NEAR, BELOW, ABOVE = pl.ds(2, 3), pl.ds(0, 2), pl.ds(5, 3)
 BF = jnp.bfloat16
@@ -251,7 +253,6 @@
 
     lax.fori_loop(2, 4, grad_step, 0)
     hop(0, 1)
-    start(quarters["near"])
     take(m_out.at[0, pl.ds(0, 3), :, YZ_COLS], g_of("by"))
     hop(1, 0)
 
@@ -263,6 +264,7 @@
 
     relay(0)
     relay(1)
+    start(quarters["near"])
     lax.fori_loop(4, 5, grad_step, 0)
     relay(2)
     hop(0, 2)
@@ -276,28 +278,36 @@
             to_partner(1, xsrc[i], ysrc[1 + k])
 
     land(0)
-    quarters_arrive(0)
-    start(acrosses["near"], wholes["near"])
     lax.fori_loop(7, 8, grad_step, 0)
     land(1)
+    hop(0, 3)
     land(2)
-    hop(0, 3)
+    quarters_arrive(0)
     land(3)
+    start(acrosses["near"], wholes["near"])
     hop(1, 1)
-    hop(2, 1)
-    start(mo)
-    take(fall.at[1 - c], g_of("ft"))
-
-    for dx in (2, 1, 3, 0):
-        q = lax.rem(x + dx, 4)
-        kind = lax.div(q, 2)
+
+    for n in range(4):
+        if n == 2:
+            hop(2, 1)
+            start(mo)
+            take(fall.at[1 - c], g_of("ft"))
+        kind = c if n < 2 else 1 - c
+        q = 2 * kind + n % 2
         basis = fall[kind].reshape(D, RANK)
         rows = pl.ds(pl.multiple_of(q * 256, 256), 256)
         low_t = jnp.dot(grad_t[rows, :], basis, preferred_element_type=F32)
         part[q] = low_t.T.astype(BF).reshape(4, 64, 256)
-        for k, (a, b) in enumerate(XY):
-            if a == dx:
-                remote(part.at[q, lax.rem(y + b, 4)], rsb.at[k], s_of("rs"), g_of("rs"), at(a, b, 0)).start()
+        a = lax.rem(q + 4 - x, 4)
+
+        def send_part(b):
+            slot = a * 4 + b - 1
+            dev = {"fs": z * 4 + lax.rem(y + b, 4), "rep": q, "tp": c}
+            remote(part.at[q, lax.rem(y + b, 4)], rsb.at[slot], s_of("rs"), g_of("rs"), dev).start()
+
+        for b in (2, 1, 3):
+            send_part(b)
+        pl.when(q != x)(functools.partial(send_part, 0))
 
     landed(0, 3)
     start(quarters["below"], quarters["above"])
@@ -461,7 +471,7 @@
     fv, nv, mv, sqv, lowv, old_v, new_v, upd_v, mom_v, mom_new, cv, s_f, s_m, s_in, s_c, s_out,
 ):
     _, y, z, _ = where_am_i()
-    order = (HERE, 2, 4, 1, 5, 0, 6, 7)
+    order = (2, 3, 4, 5, 0, 1, 6, 7)
     row = [lax.rem(z + k + 8 - HERE, 8) for k in range(8)]
     small = [
         (sq_hbm, sqv), (n_hbm, nv), (im_hbm, old_v.at[0]), (gm_hbm, old_v.at[1]), (low_hbm, lowv),
@@ -472,8 +482,9 @@
     ms = [pltpu.make_async_copy(m_hbm.at[k], mv.at[k], s_m.at[k]) for k in range(8)]
     small[0].start()
     small[1].start()
-    fs[HERE].start()
-    ms[HERE].start()
+    for k in order[:2]:
+        fs[k].start()
+        ms[k].start()
     for cp in small[2:]:
         cp.start()
     outs = []
@@ -484,7 +495,7 @@
         outs.append(cp)
 
     small[0].wait()
-    for k in order[1:]:
+    for k in order[2:]:
         fs[k].start()
         ms[k].start()
     scale = []
@@ -492,24 +503,27 @@
         square = jnp.sum(sqv[0, kind] + sqv[1, kind], axis=(0, 1), keepdims=True)
         scale.append(lax.rsqrt(square / (D * W) + 0.1))
     small[1].wait()
-    for at, k in enumerate(order):
-        fs[k].wait()
-        ms[k].wait()
+    for at, k in enumerate(order[::2]):
+        for i in (k, k + 1):
+            fs[i].wait()
+            ms[i].wait()
         for kind, out in enumerate((ic_out, gc_out)):
-            basis = fv[k, kind].reshape(256, RANK)
+            basis = fv[k : k + 2, kind].reshape(512, RANK)
             for h in range(2):
                 normed = nv[2 * kind + h].reshape(RANK, 256)
                 full = jnp.dot(basis, normed, preferred_element_type=F32)
                 col = kind * 512 + 256 * h
-                old = mv[k, :, :, col : col + 256].reshape(256, 256).astype(F32)
-                cv[k, kind, :, 256 * h : 256 * h + 256] = (old - 0.05 * (full * scale[kind])).astype(BF)
-            rows = pl.ds(pl.multiple_of(row[k] * 256, 256), 256)
-            put(cv.at[k, kind], out.at[rows, :], s_c.at[k, kind])
+                old = mv[k : k + 2, :, :, col : col + 256].reshape(512, 256).astype(F32)
+                new = (old - full * (0.05 * scale[kind])).astype(BF)
+                cv[k : k + 2, kind, :, 256 * h : 256 * h + 256] = new.reshape(2, 256, 256)
+            for i in (k, k + 1):
+                rows = pl.ds(pl.multiple_of(row[i] * 256, 256), 256)
+                put(cv.at[i, kind], out.at[rows, :], s_c.at[i, kind])
         if at == 0:
             for cp in small[2:]:
                 cp.wait()
             for kind, (new_out, upd_out) in enumerate(((im_out, iu_out), (gm_out, gu_out))):
-                basis = fv[k, kind, y].reshape(64, RANK)
+                basis = fv[HERE, kind, y].reshape(64, RANK)
                 for h in range(2):
                     normed = nv[2 * kind + h].reshape(RANK, 256)
                     cols = slice(256 * h, 256 * h + 256)

time: 66.1 us -> 63.1 us (0.955)
  Pallas kernels: 65.3 us -> 62.2 us
    pallas_call x1, Pallas kernels: 59.3 us -> 56.8 us  [gathered(): pl.pallas_call(move_kernel, name='move', out_shape=(jax.ShapeDtypeStruct(...]
where the time goes in v5:
time: 63.1 us; the launch traced here: 62.9 us
  Pallas kernels  62.2 us (99%)
  between operations  0.65 us (1%)
    pallas_call x1, Pallas kernels, gathered(): pl.pallas_call(move_kernel, name='move', out_shape=(jax.ShapeDtypeStruct(...  56.8 us
    pallas_call x1, Pallas kernels, written(): pl.pallas_call(write_kernel, name='write', out_shape=(*[jax.ShapeDtypeStr...  5.39 us

profile of v5, /device:TPU:1, one launch (start us, length us, event | category | flops | bytes accessed | tf_op | source)
XLA Modules:
  0.0 62.9 jit_solution(5724717549674500289)
XLA Ops:
  0.6 56.8 %move.1 = (bf16[8,4,64,1024]{3,2,1,0:T(8,128)(2,1)}, bf16[2,8,4,4,16,256]{5,4,3,2,1,0:T(8,128)(2,1)}, bf16[4,4,64,256]{3,2,1,0:T(8,128)(2,1)}, f32[4,8,256]{2,1,0:T(8,128)}, f32[2,2,8,128]{3,2,1,0:T(8,128)}) custom-call(bf16[1024,2048]{1,0:T(8,128)(2,1)} %x_hbm.1, bf16[1024,512]{1,0:T(8,128)(2,1)} %ci_hbm.1, bf16[1024,512]{1,0:T(8,128)(2,1)} %cg_hbm.1, ...), custom_call_target="tpu_custom_call" | custom-call | flops 6000000000 | bytes 16777216 | tf_op jit(solution)/shard_map/move/pallas_call | solution.py:422
  57.5 5.4 %write.1 = (f32[64,512]{1,0:T(8,128)}, f32[64,512]{1,0:T(8,128)}, f32[64,512]{1,0:T(8,128)}, f32[64,512]{1,0:T(8,128)}, f32[8,512]{1,0:T(8,128)}, /*index=5*/f32...) custom-call(bf16[2,8,4,4,16,256]{5,4,3,2,1,0:T(8,128)(2,1)} %get-tuple-e, ...), custom_call_target="tpu_custom_call" | custom-call | tf_op jit(solution)/shard_map/write/pallas_call | solution.py:549

commit v6 on v5

--- a/solution.py
+++ b/solution.py
@@ -11,13 +11,14 @@
 W = 1024
 RANK = 256
 NX, NY, NZ = 4, 4, 8
-YZ_COLS, YZ0, YZ1 = pl.ds(0, 384), pl.ds(0, 256), pl.ds(256, 128)
-ZY_COLS, ZYX_COLS, Z_COLS = pl.ds(384, 256), pl.ds(640, 384), pl.ds(384, 640)
+YZ_COLS, YZ0, YZ1 = pl.ds(0, 512), pl.ds(0, 256), pl.ds(256, 256)
+ZY_COLS, ZYX_COLS, Z_COLS = pl.ds(512, 128), pl.ds(640, 384), pl.ds(512, 512)
 HERE = 3
 NEAR, BELOW, ABOVE = pl.ds(2, 3), pl.ds(0, 2), pl.ds(5, 3)
 BF = jnp.bfloat16
 F32 = jnp.float32
 VMEM = 67_043_328
+KEPT = (6 * 1024 + 512 + 32 + 16) * 1024
 ANY = pl.ANY
 
 XY = sorted(
@@ -32,7 +33,7 @@
     return x, lax.rem(fs, 4), lax.div(fs, 4), c
 
 
-GROUPS = ("fz", "mo", "by", "ra", "rb", "rc", "fab", "fcd", "ft", "rs", "quarter", "whole", "across", "zs", "lo", "ag", "sq")
+GROUPS = ("fz", "mo", "by", "ra", "rb", "rc", "fab", "fcd", "ft", "rs", "quarter", "whole", "across", "zs", "lo", "nab", "ncd", "sq")
 SEM = {name: k for k, name in enumerate(GROUPS)}
 
 
@@ -53,10 +54,10 @@
 
 def move_kernel(
     x_hbm, ci_hbm, cg_hbm, im_hbm, gm_hbm, if_hbm, gf_hbm, i1_hbm, i2_hbm, g1_hbm, g2_hbm,
-    m_out, f_out, n_out, low_out, sq_out,
-    xv, cot, cot_t, grad_t, fac, fsh, fall, mast, msh, mom_in, mom_own, mom,
-    part, rsb, zb, nb, lowb, sqb,
-    s_loc, sent, got, ring_got, pair_got, land_got, leg_got,
+    m_out, fall, nb, lowb, sqb,
+    xv, cot, cot_t, grad_t, fac, fsh, mast, msh, mom_in, mom_own, mom,
+    part, rsb, zb,
+    s_loc, sent, got, ring_got, pair_got, land_got, leg_got, npair_got,
 ):
     x, y, z, c = where_am_i()
 
@@ -121,8 +122,7 @@
         cp.wait()
     msh[:, :512] = mast[0].astype(BF)
     msh[:, 512:] = mast[1].astype(BF)
-    keep_m = pltpu.make_async_copy(msh, m_out.at[HERE, y], s_loc.at[10])
-    keep_m.start()
+    m_out[HERE, y] = msh[...]
 
     pl.semaphore_wait(barrier, len(peers))
 
@@ -172,7 +172,6 @@
 
     for cp in (*fz, *by):
         cp.start()
-    keep_m.wait()
     hop(0, 0)
 
     rows16 = pl.ds(pl.multiple_of(x * 16, 16), 16)
@@ -289,7 +288,6 @@
 
     for n in range(4):
         if n == 2:
-            hop(2, 1)
             start(mo)
             take(fall.at[1 - c], g_of("ft"))
         kind = c if n < 2 else 1 - c
@@ -311,11 +309,8 @@
 
     landed(0, 3)
     start(quarters["below"], quarters["above"])
+    hop(2, 1)
     hop(1, 2)
-    hop(2, 2)
-
-    keep_f = pltpu.make_async_copy(fall, f_out, s_loc.at[11])
-    keep_f.start()
 
     grams = []
     for kind in range(2):
@@ -333,27 +328,32 @@
     zs = [remote(zb.at[z], zb.at[z], s_of("zs"), g_of("zs"), at(0, 0, d)) for k, d in enumerate(ZD)]
     for cp in zs:
         cp.start()
-    hop(1, 3)
     quarters_arrive(2)
     start(acrosses["above"])
-    hop(2, 3)
     quarters_arrive(1)
     take(mom.at[pl.ds(0, 7)], g_of("mo"))
     first = mom[:, 0].reshape(64, 256)
     second = mom[:, 1].reshape(64, 256)
     take(zb.at[pl.ds(0, 7)], g_of("zs"))
+    hop(2, 2)
+    hop(1, 3)
     low = zb[0].astype(F32)
     for k in range(1, 8):
         low = low + zb[k].astype(F32)
     first_new = 0.8 * first + 0.2 * low
     second_new = 0.95 * second + 0.05 * low * low
     nb[x, y] = (first_new / jnp.sqrt(second_new)).astype(BF)
-    ag = [
-        remote(nb.at[x, y], nb.at[x, y], s_of("ag"), g_of("ag"), at(a, b, 0))
-        for k, (a, b) in enumerate(XY)
-    ]
-    for cp in ag:
-        cp.start()
+    halves = (pl.ds(0, 32), pl.ds(32, 32))
+
+    def normed_piece(half, xs, ys, name, rsem, dev):
+        block = nb.at[xs, ys, halves[half]]
+        return remote(block, block, s_of(name), rsem, dev)
+
+    na = [normed_piece(0, x, y, "nab", npair_got.at[k], at(0, b, 0)) for k, b in enumerate(near)]
+    nbb = [normed_piece(1, x, y, "nab", npair_got.at[k], at(a, 0, 0)) for k, a in enumerate(near)]
+    nc = [[normed_piece(0, x, ys, "ncd", g_of("ncd"), at(a, 0, 0)) for a in near] for ys in ysrc]
+    nd = [[normed_piece(1, xs, y, "ncd", g_of("ncd"), at(0, b, 0)) for b in near] for xs in xsrc]
+    start(na, nbb, nc[0], nd[0])
 
     part_low = low.reshape(8, 8, 256)
     mine = jnp.zeros((8, 256), F32)
@@ -363,11 +363,13 @@
     lo = [remote(lowb.at[x], lowb.at[x], s_of("lo"), g_of("lo"), at(a, 0, 0)) for a in (2, 1, 3)]
     for cp in lo:
         cp.start()
+
+    for k in range(3):
+        take(nb.at[0, 0], npair_got.at[k])
+        start(nc[1 + k], nd[1 + k])
     start(acrosses["below"])
-
-    take(rsb, g_of("ag"))
-    keep_n = pltpu.make_async_copy(nb, n_out, s_loc.at[12])
-    keep_n.start()
+    hop(2, 3)
+    take(nb.at[pl.ds(0, 3)], g_of("ncd"))
     for kind in range(2):
         acc = jnp.zeros((8, 128), F32)
         for q in (2 * kind, 2 * kind + 1):
@@ -380,11 +382,7 @@
     sq = remote(sqb.at[c], sqb.at[c], s_of("sq"), g_of("sq"), at(0, 0, 0, 1))
     sq.start()
     take(lowb.at[pl.ds(0, 3)], g_of("lo"))
-    keep_low = pltpu.make_async_copy(lowb, low_out, s_loc.at[13])
-    keep_low.start()
     take(sqb.at[0], g_of("sq"))
-    keep_sq = pltpu.make_async_copy(sqb, sq_out, s_loc.at[14])
-    keep_sq.start()
     landed(1, 3)
     landed(2, 3)
     spread = {
@@ -406,15 +404,14 @@
         "rs": rsb,
         "quarter": m_out.at[:, pl.ds(0, 3), pl.ds(0, 16), ZYX_COLS],
         "zs": zb.at[pl.ds(0, 7)],
-        "ag": rsb,
+        "nab": nb.at[0, pl.ds(0, 3)],
+        "ncd": nb.at[pl.ds(0, 3)],
         "lo": lowb.at[pl.ds(0, 3)],
         "sq": sqb.at[0],
         **spread,
     }
     for name in GROUPS:
         take(gone[name], s_of(name))
-    for cp in (keep_f, keep_n, keep_low, keep_sq):
-        cp.wait()
 
 
 def gathered(x, ci, cg, im, gm, inf, gf, i1, i2, g1, g2):
@@ -423,14 +420,14 @@
         move_kernel,
         name="move",
         out_shape=(
-            jax.ShapeDtypeStruct((NZ, NY, 64, W), BF),
-            jax.ShapeDtypeStruct((2, NZ, NY, NX, 16, RANK), BF),
-            jax.ShapeDtypeStruct((NX, NY, 64, 256), BF),
-            jax.ShapeDtypeStruct((NX, 8, 256), F32),
-            jax.ShapeDtypeStruct((2, 2, 8, 128), F32),
+            pltpu.VMEM((NZ, NY, 64, W), BF),
+            pltpu.VMEM((2, NZ, NY, NX, 16, RANK), BF),
+            pltpu.VMEM((NX, NY, 64, 256), BF),
+            pltpu.VMEM((NX, 8, 256), F32),
+            pltpu.VMEM((2, 2, 8, 128), F32),
         ),
         in_specs=[pl.BlockSpec(memory_space=ANY)] * 11,
-        out_specs=[pl.BlockSpec(memory_space=ANY)] * 5,
+        out_specs=[pl.BlockSpec(memory_space=pltpu.VMEM)] * 5,
         scratch_shapes=[
             pltpu.VMEM((1024, D), BF),
             pltpu.VMEM((2, 1024, 512), BF),
@@ -438,7 +435,6 @@
             pltpu.VMEM((1024, D), BF),
             pltpu.VMEM((64, RANK), BF),
             pltpu.VMEM((4, 16, RANK), BF),
-            pltpu.VMEM((2, NZ, NY, NX, 16, RANK), BF),
             pltpu.VMEM((2, 64, 512), F32),
             pltpu.VMEM((64, W), BF),
             pltpu.VMEM((4, 8, 512), F32),
@@ -447,45 +443,36 @@
             pltpu.VMEM((NX, NY, 64, 256), BF),
             pltpu.VMEM((15, 64, 256), BF),
             pltpu.VMEM((NZ, 64, 256), BF),
-            pltpu.VMEM((NX, NY, 64, 256), BF),
-            pltpu.VMEM((NX, 8, 256), F32),
-            pltpu.VMEM((2, 2, 8, 128), F32),
-            sem((15,)),
+            sem((10,)),
             sem((len(GROUPS),)),
             sem((len(GROUPS),)),
             sem((3, 4)),
             sem((3,)),
             sem((4,)),
             sem((3,)),
+            sem((3,)),
         ],
         compiler_params=pltpu.CompilerParams(
-            collective_id=0, has_side_effects=True, vmem_limit_bytes=VMEM
+            collective_id=0, has_side_effects=True, vmem_limit_bytes=VMEM - KEPT
         ),
         cost_estimate=pl.CostEstimate(flops=6 * 10**9, bytes_accessed=16 * 2**20, transcendentals=0),
     )(x, ci, cg, im, gm, inf, gf, i1, i2, g1, g2)
 
 
 def write_kernel(
-    f_hbm, n_hbm, m_hbm, sq_hbm, low_hbm, im_hbm, gm_hbm, i1_hbm, i2_hbm, g1_hbm, g2_hbm,
+    fv, nv, mv, sqv, lowv, im_hbm, gm_hbm, i1_hbm, i2_hbm, g1_hbm, g2_hbm,
     im_out, gm_out, iu_out, gu_out, i1_out, i2_out, g1_out, g2_out, ic_out, gc_out,
-    fv, nv, mv, sqv, lowv, old_v, new_v, upd_v, mom_v, mom_new, cv, s_f, s_m, s_in, s_c, s_out,
+    old_v, new_v, upd_v, mom_v, mom_new, cv, s_in, s_c, s_out,
 ):
     _, y, z, _ = where_am_i()
     order = (2, 3, 4, 5, 0, 1, 6, 7)
     row = [lax.rem(z + k + 8 - HERE, 8) for k in range(8)]
     small = [
-        (sq_hbm, sqv), (n_hbm, nv), (im_hbm, old_v.at[0]), (gm_hbm, old_v.at[1]), (low_hbm, lowv),
+        (im_hbm, old_v.at[0]), (gm_hbm, old_v.at[1]),
         *[(r, mom_v.at[k]) for k, r in enumerate((i1_hbm, i2_hbm, g1_hbm, g2_hbm))],
     ]
     small = [pltpu.make_async_copy(src, dst, s_in.at[k]) for k, (src, dst) in enumerate(small)]
-    fs = [pltpu.make_async_copy(f_hbm.at[:, row[k]], fv.at[k], s_f.at[k]) for k in range(8)]
-    ms = [pltpu.make_async_copy(m_hbm.at[k], mv.at[k], s_m.at[k]) for k in range(8)]
-    small[0].start()
-    small[1].start()
-    for k in order[:2]:
-        fs[k].start()
-        ms[k].start()
-    for cp in small[2:]:
+    for cp in small:
         cp.start()
     outs = []
 
@@ -494,21 +481,13 @@
         cp.start()
         outs.append(cp)
 
-    small[0].wait()
-    for k in order[2:]:
-        fs[k].start()
-        ms[k].start()
     scale = []
     for kind in range(2):
         square = jnp.sum(sqv[0, kind] + sqv[1, kind], axis=(0, 1), keepdims=True)
         scale.append(lax.rsqrt(square / (D * W) + 0.1))
-    small[1].wait()
     for at, k in enumerate(order[::2]):
-        for i in (k, k + 1):
-            fs[i].wait()
-            ms[i].wait()
         for kind, out in enumerate((ic_out, gc_out)):
-            basis = fv[k : k + 2, kind].reshape(512, RANK)
+            basis = jnp.concatenate([fv[kind, row[i]].reshape(256, RANK) for i in (k, k + 1)], axis=0)
             for h in range(2):
                 normed = nv[2 * kind + h].reshape(RANK, 256)
                 full = jnp.dot(basis, normed, preferred_element_type=F32)
@@ -520,10 +499,10 @@
                 rows = pl.ds(pl.multiple_of(row[i] * 256, 256), 256)
                 put(cv.at[i, kind], out.at[rows, :], s_c.at[i, kind])
         if at == 0:
-            for cp in small[2:]:
+            for cp in small:
                 cp.wait()
             for kind, (new_out, upd_out) in enumerate(((im_out, iu_out), (gm_out, gu_out))):
-                basis = fv[HERE, kind, y].reshape(64, RANK)
+                basis = fv[kind, z, y].reshape(64, RANK)
                 for h in range(2):
                     normed = nv[2 * kind + h].reshape(RANK, 256)
                     cols = slice(256 * h, 256 * h + 256)
@@ -546,6 +525,7 @@
 
 def written(f, n, m, sq, low, im, gm, i1, i2, g1, g2):
     sem, kept = pltpu.SemaphoreType.DMA, pl.BlockSpec(memory_space=ANY)
+    held = pl.BlockSpec(memory_space=pltpu.VMEM)
     return pl.pallas_call(
         write_kernel,
         name="write",
@@ -554,27 +534,23 @@
             *[jax.ShapeDtypeStruct((8, 512), F32)] * 4,
             *[jax.ShapeDtypeStruct((D, 512), BF)] * 2,
         ),
-        in_specs=[kept] * 11,
+        in_specs=[held] * 5 + [kept] * 6,
         out_specs=[kept] * 10,
         scratch_shapes=[
-            pltpu.VMEM((8, 2, NY, NX, 16, RANK), BF),
-            pltpu.VMEM((NX, NY, 64, 256), BF),
-            pltpu.VMEM((8, NY, 64, W), BF),
-            pltpu.VMEM((2, 2, 8, 128), F32),
-            pltpu.VMEM((NX, 8, 256), F32),
             *[pltpu.VMEM((2, 64, 512), F32)] * 3,
             *[pltpu.VMEM((4, 8, 512), F32)] * 2,
             pltpu.VMEM((8, 2, 256, 512), BF),
-            *[sem((n,)) for n in (8, 8, 9)],
+            sem((6,)),
             sem((8, 2)),
             sem((8,)),
         ],
-        compiler_params=pltpu.CompilerParams(vmem_limit_bytes=VMEM),
+        compiler_params=pltpu.CompilerParams(vmem_limit_bytes=VMEM - KEPT),
     )(f, n, m, sq, low, im, gm, i1, i2, g1, g2)
 
 
 def on_device(x, ci, cg, im, gm, inf, gf, i1, i2, g1, g2):
     m, f, n, low, sq = gathered(x, ci, cg, im, gm, inf, gf, i1, i2, g1, g2)
+    f, n, m, sq, low = (pltpu.with_memory_space_constraint(a, pltpu.VMEM) for a in (f, n, m, sq, low))
     out = written(f, n, m, sq, low, im, gm, i1, i2, g1, g2)
     return tuple(out)
 

time: 63.1 us -> 62.5 us (level)
    pallas_call x1, Pallas kernels: 5.39 us -> 4.02 us  [written(): pl.pallas_call(write_kernel, name='write', out_shape=(*[jax.ShapeDtypeStr...]
    pallas_call x1, Pallas kernels: 56.8 us -> 57.7 us  [gathered(): pl.pallas_call(move_kernel, name='move', out_shape=(pltpu.VMEM((NZ, NY, 6...]
where the time goes in v6:
time: 62.5 us; the launch traced here: 62.4 us
  Pallas kernels  61.8 us (99%)
  between operations  0.65 us (1%)
    pallas_call x1, Pallas kernels, gathered(): pl.pallas_call(move_kernel, name='move', out_shape=(pltpu.VMEM((NZ, NY, 6...  57.7 us
    pallas_call x1, Pallas kernels, written(): pl.pallas_call(write_kernel, name='write', out_shape=(*[jax.ShapeDtypeStr...  4.02 us

profile of v6, /device:TPU:1, one launch (start us, length us, event | category | flops | bytes accessed | tf_op | source)
XLA Modules:
  0.0 62.4 jit_solution(1011685988178168223)
XLA Ops:
  0.6 57.7 %move.1 = (bf16[8,4,64,1024]{3,2,1,0:T(8,128)(2,1)S(1)}, bf16[2,8,4,4,16,256]{5,4,3,2,1,0:T(8,128)(2,1)S(1)}, bf16[4,4,64,256]{3,2,1,0:T(8,128)(2,1)S(1)}, f32[4,8,256]{2,1,0:T(8,128)S(1)}, f32[2,2,8,128]{3,2,1,0:T(8,128)S(1)}) custom-call(bf16[1024,2048]{1,0:T(8,128)(2,1)} %x_hbm.1, bf16[1024,512]{1,0:T(8,128)(2,1)} %ci_hbm.1, bf16[1024,512]{1,0:T(8,128)(2,1)} %cg_hbm.1, ...), custom_call_target="tpu_custom_call" | custom-call | flops 6000000000 | bytes 16777216 | tf_op jit(solution)/shard_map/move/pallas_call | solution.py:419
  58.4 4.0 %write.1 = (f32[64,512]{1,0:T(8,128)}, f32[64,512]{1,0:T(8,128)}, f32[64,512]{1,0:T(8,128)}, f32[64,512]{1,0:T(8,128)}, f32[8,512]{1,0:T(8,128)}, /*index=5*/f32...) custom-call(bf16[2,8,4,4,16,256]{5,4,3,2,1,0:T(8,128)(2,1)S(1)} %get-tup, ...), custom_call_target="tpu_custom_call" | custom-call | tf_op jit(solution)/shard_map/write/pallas_call | solution.py:529

commit v7 on v6

--- a/solution.py
+++ b/solution.py
@@ -465,8 +465,6 @@
     old_v, new_v, upd_v, mom_v, mom_new, cv, s_in, s_c, s_out,
 ):
     _, y, z, _ = where_am_i()
-    order = (2, 3, 4, 5, 0, 1, 6, 7)
-    row = [lax.rem(z + k + 8 - HERE, 8) for k in range(8)]
     small = [
         (im_hbm, old_v.at[0]), (gm_hbm, old_v.at[1]),
         *[(r, mom_v.at[k]) for k, r in enumerate((i1_hbm, i2_hbm, g1_hbm, g2_hbm))],
@@ -485,42 +483,55 @@
     for kind in range(2):
         square = jnp.sum(sqv[0, kind] + sqv[1, kind], axis=(0, 1), keepdims=True)
         scale.append(lax.rsqrt(square / (D * W) + 0.1))
-    for at, k in enumerate(order[::2]):
-        for kind, out in enumerate((ic_out, gc_out)):
-            basis = jnp.concatenate([fv[kind, row[i]].reshape(256, RANK) for i in (k, k + 1)], axis=0)
+
+    def rows_out(b, kind):
+        out = (ic_out, gc_out)[kind]
+        rows = pl.ds(pl.multiple_of(256 * b, 256), 256)
+        return pltpu.make_async_copy(cv.at[b, kind], out.at[rows, :], s_c.at[b, kind])
+
+    def blocks(p, _):
+        k = 2 * p
+        for kind in range(2):
+            basis = fv[kind, pl.ds(k, 2)].reshape(512, RANK)
             for h in range(2):
                 normed = nv[2 * kind + h].reshape(RANK, 256)
                 full = jnp.dot(basis, normed, preferred_element_type=F32)
                 col = kind * 512 + 256 * h
-                old = mv[k : k + 2, :, :, col : col + 256].reshape(512, 256).astype(F32)
-                new = (old - full * (0.05 * scale[kind])).astype(BF)
-                cv[k : k + 2, kind, :, 256 * h : 256 * h + 256] = new.reshape(2, 256, 256)
-            for i in (k, k + 1):
-                rows = pl.ds(pl.multiple_of(row[i] * 256, 256), 256)
-                put(cv.at[i, kind], out.at[rows, :], s_c.at[i, kind])
-        if at == 0:
-            for cp in small:
-                cp.wait()
-            for kind, (new_out, upd_out) in enumerate(((im_out, iu_out), (gm_out, gu_out))):
-                basis = fv[kind, z, y].reshape(64, RANK)
-                for h in range(2):
-                    normed = nv[2 * kind + h].reshape(RANK, 256)
-                    cols = slice(256 * h, 256 * h + 256)
-                    u = jnp.dot(basis, normed, preferred_element_type=F32) * scale[kind]
-                    upd_v[kind, :, cols] = u
-                    new_v[kind, :, cols] = old_v[kind, :, cols] - 0.05 * u
-                put(upd_v.at[kind], upd_out, s_out.at[2 * kind])
-                put(new_v.at[kind], new_out, s_out.at[2 * kind + 1])
-            for kind, (first_out, second_out) in enumerate(((i1_out, i2_out), (g1_out, g2_out))):
-                for h in range(2):
-                    low = lowv[2 * kind + h]
-                    cols = slice(256 * h, 256 * h + 256)
-                    mom_new[2 * kind, :, cols] = 0.8 * mom_v[2 * kind, :, cols] + 0.2 * low
-                    mom_new[2 * kind + 1, :, cols] = 0.95 * mom_v[2 * kind + 1, :, cols] + 0.05 * low * low
-                put(mom_new.at[2 * kind], first_out, s_out.at[4 + 2 * kind])
-                put(mom_new.at[2 * kind + 1], second_out, s_out.at[5 + 2 * kind])
+                for i in range(2):
+                    old = mv[lax.rem(k + i + 8 - z + HERE, 8), :, :, col : col + 256].reshape(256, 256)
+                    new = old.astype(F32) - full[256 * i : 256 * (i + 1)] * (0.05 * scale[kind])
+                    cv[k + i, kind, :, 256 * h : 256 * h + 256] = new.astype(BF)
+            for i in range(2):
+                rows_out(k + i, kind).start()
+        return 0
+
+    lax.fori_loop(0, 2, blocks, 0)
+    for cp in small:
+        cp.wait()
+    for kind, (new_out, upd_out) in enumerate(((im_out, iu_out), (gm_out, gu_out))):
+        basis = fv[kind, z, y].reshape(64, RANK)
+        for h in range(2):
+            normed = nv[2 * kind + h].reshape(RANK, 256)
+            cols = slice(256 * h, 256 * h + 256)
+            u = jnp.dot(basis, normed, preferred_element_type=F32) * scale[kind]
+            upd_v[kind, :, cols] = u
+            new_v[kind, :, cols] = old_v[kind, :, cols] - 0.05 * u
+        put(upd_v.at[kind], upd_out, s_out.at[2 * kind])
+        put(new_v.at[kind], new_out, s_out.at[2 * kind + 1])
+    for kind, (first_out, second_out) in enumerate(((i1_out, i2_out), (g1_out, g2_out))):
+        for h in range(2):
+            low = lowv[2 * kind + h]
+            cols = slice(256 * h, 256 * h + 256)
+            mom_new[2 * kind, :, cols] = 0.8 * mom_v[2 * kind, :, cols] + 0.2 * low
+            mom_new[2 * kind + 1, :, cols] = 0.95 * mom_v[2 * kind + 1, :, cols] + 0.05 * low * low
+        put(mom_new.at[2 * kind], first_out, s_out.at[4 + 2 * kind])
+        put(mom_new.at[2 * kind + 1], second_out, s_out.at[5 + 2 * kind])
+    lax.fori_loop(2, 4, blocks, 0)
     for cp in outs:
         cp.wait()
+    for b in range(8):
+        for kind in range(2):
+            rows_out(b, kind).wait()
 
 
 def written(f, n, m, sq, low, im, gm, i1, i2, g1, g2):

time: 62.5 us -> 61.7 us (0.987)
  Pallas kernels: 61.8 us -> 61 us
    pallas_call x1, Pallas kernels: 4.02 us -> 3.22 us  [written(): pl.pallas_call(write_kernel, name='write', out_shape=(*[jax.ShapeDtypeStr...]
where the time goes in v7:
time: 61.7 us; the launch traced here: 61.6 us
  Pallas kernels  61 us (99%)
  between operations  0.65 us (1%)
    pallas_call x1, Pallas kernels, gathered(): pl.pallas_call(move_kernel, name='move', out_shape=(pltpu.VMEM((NZ, NY, 6...  57.7 us
    pallas_call x1, Pallas kernels, written(): pl.pallas_call(write_kernel, name='write', out_shape=(*[jax.ShapeDtypeStr...  3.22 us

profile of v7, /device:TPU:1, one launch (start us, length us, event | category | flops | bytes accessed | tf_op | source)
XLA Modules:
  0.0 61.6 jit_solution(1047853048119180720)
XLA Ops:
  0.6 57.7 %move.1 = (bf16[8,4,64,1024]{3,2,1,0:T(8,128)(2,1)S(1)}, bf16[2,8,4,4,16,256]{5,4,3,2,1,0:T(8,128)(2,1)S(1)}, bf16[4,4,64,256]{3,2,1,0:T(8,128)(2,1)S(1)}, f32[4,8,256]{2,1,0:T(8,128)S(1)}, f32[2,2,8,128]{3,2,1,0:T(8,128)S(1)}) custom-call(bf16[1024,2048]{1,0:T(8,128)(2,1)} %x_hbm.1, bf16[1024,512]{1,0:T(8,128)(2,1)} %ci_hbm.1, bf16[1024,512]{1,0:T(8,128)(2,1)} %cg_hbm.1, ...), custom_call_target="tpu_custom_call" | custom-call | flops 6000000000 | bytes 16777216 | tf_op jit(solution)/shard_map/move/pallas_call | solution.py:419
  58.4 3.2 %write.1 = (f32[64,512]{1,0:T(8,128)}, f32[64,512]{1,0:T(8,128)}, f32[64,512]{1,0:T(8,128)}, f32[64,512]{1,0:T(8,128)}, f32[8,512]{1,0:T(8,128)}, /*index=5*/f32...) custom-call(bf16[2,8,4,4,16,256]{5,4,3,2,1,0:T(8,128)(2,1)S(1)} %get-tup, ...), custom_call_target="tpu_custom_call" | custom-call | tf_op jit(solution)/shard_map/write/pallas_call | solution.py:540

commit v8 on v7

--- a/solution.py
+++ b/solution.py
@@ -35,6 +35,7 @@
 
 GROUPS = ("fz", "mo", "by", "ra", "rb", "rc", "fab", "fcd", "ft", "rs", "quarter", "whole", "across", "zs", "lo", "nab", "ncd", "sq")
 SEM = {name: k for k, name in enumerate(GROUPS)}
+GOT = {name: k for k, name in enumerate(("fz", "mo", "by", "ft", "rs", "whole", "across", "zs", "lo", "ncd", "sq"))}
 
 
 def take(region, sem):
@@ -72,7 +73,7 @@
         return sent.at[SEM[name]]
 
     def g_of(name):
-        return got.at[SEM[name]]
+        return got.at[GOT[name]]
 
     @pl.when(c == 0)
     def _():
@@ -286,26 +287,24 @@
     start(acrosses["near"], wholes["near"])
     hop(1, 1)
 
-    for n in range(4):
-        if n == 2:
+    def send_part(q, a, b):
+        dev = {"fs": z * 4 + lax.rem(y + b, 4), "rep": q, "tp": c}
+        slot = rsb.at[a * 4 + b - 1]
+        remote(part.at[q, lax.rem(y + b, 4)], slot, s_of("rs"), g_of("rs"), dev).start()
+
+    for kind in (c, 1 - c):
+        if kind is not c:
             start(mo)
             take(fall.at[1 - c], g_of("ft"))
-        kind = c if n < 2 else 1 - c
-        q = 2 * kind + n % 2
-        basis = fall[kind].reshape(D, RANK)
-        rows = pl.ds(pl.multiple_of(q * 256, 256), 256)
-        low_t = jnp.dot(grad_t[rows, :], basis, preferred_element_type=F32)
-        part[q] = low_t.T.astype(BF).reshape(4, 64, 256)
-        a = lax.rem(q + 4 - x, 4)
-
-        def send_part(b):
-            slot = a * 4 + b - 1
-            dev = {"fs": z * 4 + lax.rem(y + b, 4), "rep": q, "tp": c}
-            remote(part.at[q, lax.rem(y + b, 4)], rsb.at[slot], s_of("rs"), g_of("rs"), dev).start()
-
-        for b in (2, 1, 3):
-            send_part(b)
-        pl.when(q != x)(functools.partial(send_part, 0))
+        rows = pl.ds(pl.multiple_of(kind * 512, 512), 512)
+        low_t = jnp.dot(grad_t[rows, :], fall[kind].reshape(D, RANK), preferred_element_type=F32)
+        for h in range(2):
+            q = 2 * kind + h
+            part[q] = low_t[256 * h : 256 * (h + 1)].astype(BF).T.reshape(4, 64, 256)
+            a = lax.rem(q + 4 - x, 4)
+            for b in (2, 1, 3):
+                send_part(q, a, b)
+            pl.when(q != x)(functools.partial(send_part, q, a, 0))
 
     landed(0, 3)
     start(quarters["below"], quarters["above"])
@@ -445,7 +444,7 @@
             pltpu.VMEM((NZ, 64, 256), BF),
             sem((10,)),
             sem((len(GROUPS),)),
-            sem((len(GROUPS),)),
+            sem((len(GOT),)),
             sem((3, 4)),
             sem((3,)),
             sem((4,)),

time: 61.7 us -> 60.8 us (0.985)
  Pallas kernels: 61 us -> 60.1 us
    pallas_call x1, Pallas kernels: 57.7 us -> 56.9 us  [gathered(): pl.pallas_call(move_kernel, name='move', out_shape=(pltpu.VMEM((NZ, NY, 6...]
where the time goes in v8:
time: 60.8 us; the launch traced here: 60.7 us
  Pallas kernels  60.1 us (99%)
  between operations  0.65 us (1%)
    pallas_call x1, Pallas kernels, gathered(): pl.pallas_call(move_kernel, name='move', out_shape=(pltpu.VMEM((NZ, NY, 6...  56.9 us
    pallas_call x1, Pallas kernels, written(): pl.pallas_call(write_kernel, name='write', out_shape=(*[jax.ShapeDtypeStr...  3.22 us

profile of v8, /device:TPU:1, one launch (start us, length us, event | category | flops | bytes accessed | tf_op | source)
XLA Modules:
  0.0 60.7 jit_solution(12144072302374690199)
XLA Ops:
  0.6 56.9 %move.1 = (bf16[8,4,64,1024]{3,2,1,0:T(8,128)(2,1)S(1)}, bf16[2,8,4,4,16,256]{5,4,3,2,1,0:T(8,128)(2,1)S(1)}, bf16[4,4,64,256]{3,2,1,0:T(8,128)(2,1)S(1)}, f32[4,8,256]{2,1,0:T(8,128)S(1)}, f32[2,2,8,128]{3,2,1,0:T(8,128)S(1)}) custom-call(bf16[1024,2048]{1,0:T(8,128)(2,1)} %x_hbm.1, bf16[1024,512]{1,0:T(8,128)(2,1)} %ci_hbm.1, bf16[1024,512]{1,0:T(8,128)(2,1)} %cg_hbm.1, ...), custom_call_target="tpu_custom_call" | custom-call | flops 6000000000 | bytes 16777216 | tf_op jit(solution)/shard_map/move/pallas_call | solution.py:418
  57.5 3.2 %write.1 = (f32[64,512]{1,0:T(8,128)}, f32[64,512]{1,0:T(8,128)}, f32[64,512]{1,0:T(8,128)}, f32[64,512]{1,0:T(8,128)}, f32[8,512]{1,0:T(8,128)}, /*index=5*/f32...) custom-call(bf16[2,8,4,4,16,256]{5,4,3,2,1,0:T(8,128)(2,1)S(1)} %get-tup, ...), custom_call_target="tpu_custom_call" | custom-call | tf_op jit(solution)/shard_map/write/pallas_call | solution.py:539

commit v9 on v8

--- a/solution.py
+++ b/solution.py
@@ -174,6 +174,8 @@
     for cp in (*fz, *by):
         cp.start()
     hop(0, 0)
+    for cp in mo:
+        cp.start()
 
     rows16 = pl.ds(pl.multiple_of(x * 16, 16), 16)
     part_of = {"near": NEAR, "below": BELOW, "above": ABOVE}
@@ -294,7 +296,6 @@
 
     for kind in (c, 1 - c):
         if kind is not c:
-            start(mo)
             take(fall.at[1 - c], g_of("ft"))
         rows = pl.ds(pl.multiple_of(kind * 512, 512), 512)
         low_t = jnp.dot(grad_t[rows, :], fall[kind].reshape(D, RANK), preferred_element_type=F32)

time: 60.8 us -> 60 us (0.987)
  Pallas kernels: 60.1 us -> 59.3 us
    pallas_call x1, Pallas kernels: 56.9 us -> 56 us  [gathered(): pl.pallas_call(move_kernel, name='move', out_shape=(pltpu.VMEM((NZ, NY, 6...]
where the time goes in v9:
time: 60 us; the launch traced here: 59.9 us
  Pallas kernels  59.3 us (99%)
  between operations  0.65 us (1%)
    pallas_call x1, Pallas kernels, gathered(): pl.pallas_call(move_kernel, name='move', out_shape=(pltpu.VMEM((NZ, NY, 6...  56 us
    pallas_call x1, Pallas kernels, written(): pl.pallas_call(write_kernel, name='write', out_shape=(*[jax.ShapeDtypeStr...  3.22 us

profile of v9, /device:TPU:1, one launch (start us, length us, event | category | flops | bytes accessed | tf_op | source)
XLA Modules:
  0.0 59.9 jit_solution(8359624584239518114)
XLA Ops:
  0.6 56.0 %move.1 = (bf16[8,4,64,1024]{3,2,1,0:T(8,128)(2,1)S(1)}, bf16[2,8,4,4,16,256]{5,4,3,2,1,0:T(8,128)(2,1)S(1)}, bf16[4,4,64,256]{3,2,1,0:T(8,128)(2,1)S(1)}, f32[4,8,256]{2,1,0:T(8,128)S(1)}, f32[2,2,8,128]{3,2,1,0:T(8,128)S(1)}) custom-call(bf16[1024,2048]{1,0:T(8,128)(2,1)} %x_hbm.1, bf16[1024,512]{1,0:T(8,128)(2,1)} %ci_hbm.1, bf16[1024,512]{1,0:T(8,128)(2,1)} %cg_hbm.1, ...), custom_call_target="tpu_custom_call" | custom-call | flops 6000000000 | bytes 16777216 | tf_op jit(solution)/shard_map/move/pallas_call | solution.py:419
  56.7 3.2 %write.1 = (f32[64,512]{1,0:T(8,128)}, f32[64,512]{1,0:T(8,128)}, f32[64,512]{1,0:T(8,128)}, f32[64,512]{1,0:T(8,128)}, f32[8,512]{1,0:T(8,128)}, /*index=5*/f32...) custom-call(bf16[2,8,4,4,16,256]{5,4,3,2,1,0:T(8,128)(2,1)S(1)} %get-tup, ...), custom_call_target="tpu_custom_call" | custom-call | tf_op jit(solution)/shard_map/write/pallas_call | solution.py:540
